TPU v7x, 768 devices: a whole 4x8x12 slice. The times are simulated.
768 devices in a mesh: sp: 48 (over z, x), tp: 16 (over y, core).
Axes of the slice: x: 4, y: 8, z: 12, core: 2. Of those that a mesh axis runs over, the one named last changes fastest.
Arguments:
- grid_in: bfloat16 [6144, 2048], P('sp', 'tp'), may hold values from -6 to 6
- documents: int32 [6144], P('sp'), may hold values from 0 to 23, never falling along the last dimension, each value on 1 to 512 neighbouring positions
- pre_gain: float32 [2, 2048], replicated, may hold values from 0.1 to 1.9
- query_weight: bfloat16 [2, 2048, 2048], P(None, None, 'tp'), may hold values from -1 to 1
- key_weight: bfloat16 [2, 2048, 2048], P(None, None, 'tp'), may hold values from -4 to 4
- value_weight: bfloat16 [2, 2048, 2048], P(None, None, 'tp'), may hold values from -0.125 to 0.125
- offset_bias: float32 [2, 32, 15, 31], P(None, 'tp'), may hold values from -5 to 5
- out_weight: bfloat16 [2, 2048, 2048], P(None, None, 'tp'), may hold values from -3 to 3
- post_gain: float32 [2, 2048], P(None, 'tp'), may hold values from 0.1 to 1.9
Outputs:
- grid_out: bfloat16 [6144, 2048], P('sp', 'tp')
Inputs may be any that keep to these rules, and one draw needn't show every extreme that they name: `documents`: each position's document number; numbers never fall along the token order, and each document covers 1 to 512 positions.
All inputs are finite; a program needn't handle non-finite values.
Results may differ from a plain program's by a relative error of at most 0.0095.
Values may be sent and summed in bfloat16 or wider, within the bound.
No kernel may reach another device: no remote copies, remote signals or barrier semaphores. Data moves between devices by JAX's collectives and lax.ppermute only.
A program may use at most 64 MiB of HBM per device.

v0:
```python
import jax
import jax.numpy as jnp
from jax import lax
from jax.sharding import PartitionSpec as P

HEAD_DIM = 64
WIN_ROWS = 8
WIN_COLS = 16
GRID_W = 32
LAYERS = 2


epsilon = 1e-06


def in_order(parts, dim):
    parts = jnp.moveaxis(parts, 0, dim)
    shape = parts.shape
    return parts.reshape(*shape[:dim], shape[dim] * shape[dim + 1], *shape[dim + 2 :])


def from_everyone(array, axis):
    length = lax.axis_size(axis)
    return lax.all_to_all(
        jnp.broadcast_to(array[None], (length, *array.shape)), axis, 0, 0, tiled=True
    )


def collect(array, axis, dim):
    return in_order(from_everyone(array, axis), dim)


def extended(block, sides, width):
    for axis, dim in sides:
        count = lax.axis_size(axis)
        forward = [(i, i + 1) for i in range(count - 1)]
        backward = [(target, source) for source, target in forward]
        low = lax.ppermute(
            lax.slice_in_dim(block, block.shape[dim] - width, None, axis=dim), axis, forward
        )
        high = lax.ppermute(lax.slice_in_dim(block, 0, width, axis=dim), axis, backward)
        block = jnp.concatenate([low, block, high], axis=dim)
    return block


def of_everyone(array, axis):
    return from_everyone(array, axis).sum(axis=0)


def project(rows_in, own_from, own_count, gain_row, query_part, key_part, value_part):
    model_width = gain_row.shape[0]
    widened = collect(rows_in, "tp", 1).astype(jnp.float32)
    scaled = (widened * gain_row[None, :]).astype(jnp.bfloat16)
    query_sum = jnp.dot(scaled, query_part, preferred_element_type=jnp.float32)
    key_sum = jnp.dot(scaled, key_part, preferred_element_type=jnp.float32)
    value_sum = jnp.dot(scaled, value_part, preferred_element_type=jnp.float32)
    squares = jnp.sum(widened * widened, axis=1)
    scaler = lax.rsqrt(squares / model_width + epsilon)[:, None]
    return (
        (query_sum * scaler).astype(jnp.bfloat16),
        (key_sum * scaler).astype(jnp.bfloat16),
        (value_sum * scaler).astype(jnp.bfloat16),
    )


def shards(
    grid_in,
    documents,
    pre_gain,
    query_weight,
    key_weight,
    value_weight,
    offset_bias,
    out_weight,
    post_gain,
):
    tokens_here, feat_here = grid_in.shape
    model_width = pre_gain.shape[1]
    head_count = offset_bias.shape[1]
    head_cols = query_weight.shape[2]
    row_count = tokens_here // GRID_W
    all_rows = row_count * lax.axis_size("sp")
    rim_rows = WIN_ROWS // 2
    first_row = lax.axis_index("sp") * row_count
    global_rows = first_row + jnp.arange(row_count, dtype=jnp.int32)
    slab_start = jnp.clip(global_rows - rim_rows, 0, all_rows - WIN_ROWS)
    window_rows = jnp.arange(WIN_ROWS, dtype=jnp.int32)
    slab_index = (slab_start - first_row + rim_rows)[:, None] + window_rows[None, :]
    row_offset = slab_start[:, None] + window_rows[None, :] - global_rows[:, None] + WIN_ROWS - 1
    row_onehot = (
        row_offset[:, :, None] == jnp.arange(2 * WIN_ROWS - 1, dtype=jnp.int32)[None, None, :]
    ).astype(jnp.float32)
    columns = jnp.arange(GRID_W, dtype=jnp.int32)
    col_start = jnp.clip(columns - WIN_COLS // 2, 0, GRID_W - WIN_COLS)
    col_allowed = (columns[None, :] >= col_start[:, None]) & (
        columns[None, :] < col_start[:, None] + WIN_COLS
    )
    col_offset = columns[None, :] - columns[:, None] + WIN_COLS - 1
    col_onehot = (
        (col_offset[:, :, None] == jnp.arange(2 * WIN_COLS - 1, dtype=jnp.int32)[None, None, :])
        & col_allowed[:, :, None]
    ).astype(jnp.float32)
    own_docs = documents.reshape(row_count, GRID_W)
    score_scale = HEAD_DIM ** (-0.5)
    stream = grid_in
    for layer_index in range(LAYERS):
        weights_here = (
            pre_gain[layer_index],
            query_weight[layer_index],
            key_weight[layer_index],
            value_weight[layer_index],
        )
        query_rows, key_rows, value_rows = project(stream, 0, tokens_here, *weights_here)
        key_wide, value_wide, wide_docs = (
            extended(key_rows.reshape(row_count, GRID_W, head_cols), (("sp", 0),), rim_rows),
            extended(value_rows.reshape(row_count, GRID_W, head_cols), (("sp", 0),), rim_rows),
            extended(own_docs, (("sp", 0),), rim_rows),
        )
        key_slab = jnp.take(key_wide, slab_index, axis=0).reshape(
            row_count, WIN_ROWS, GRID_W, head_count, HEAD_DIM
        )
        value_slab = jnp.take(value_wide, slab_index, axis=0).reshape(
            row_count, WIN_ROWS, GRID_W, head_count, HEAD_DIM
        )
        doc_slab = jnp.take(wide_docs, slab_index, axis=0)
        query_grid = query_rows.reshape(row_count, GRID_W, head_count, HEAD_DIM)
        bias_grid = jnp.einsum(
            "hrt,ijr,ckt->ihcjk",
            offset_bias[layer_index],
            row_onehot,
            col_onehot,
            precision=lax.Precision.HIGHEST,
        )
        scores = (
            jnp.einsum(
                "ichd,ijkhd->ihcjk", query_grid, key_slab, preferred_element_type=jnp.float32
            )
            * score_scale
            + bias_grid
        )
        allowed = (doc_slab[:, None, :, :] == own_docs[:, :, None, None]) & col_allowed[
            None, :, None, :
        ]
        scores = jnp.where(allowed[:, None], scores, -jnp.inf)
        row_peak = jnp.max(scores, axis=(3, 4), keepdims=True)
        lifted = jnp.exp(scores - row_peak)
        weights = (lifted / jnp.sum(lifted, axis=(3, 4), keepdims=True)).astype(jnp.bfloat16)
        attended = jnp.einsum(
            "ihcjk,ijkhd->ichd", weights, value_slab, preferred_element_type=jnp.float32
        )
        attended = attended.astype(jnp.bfloat16).reshape(tokens_here, head_cols)
        out_here = out_weight[layer_index]
        branch = jnp.dot(collect(attended, "tp", 1), out_here, preferred_element_type=jnp.float32)
        branch_total = of_everyone(jnp.sum(branch * branch, axis=1), "tp")
        branch_scale = lax.rsqrt(branch_total / model_width + epsilon)[:, None]
        stream = (
            stream.astype(jnp.float32) + branch * branch_scale * post_gain[layer_index][None, :]
        ).astype(jnp.bfloat16)
    return stream


def solution(mesh):
    return jax.shard_map(
        shards,
        mesh=mesh,
        in_specs=(
            P("sp", "tp"),
            P("sp"),
            P(),
            P(None, None, "tp"),
            P(None, None, "tp"),
            P(None, None, "tp"),
            P(None, "tp", None, None),
            P(None, None, "tp"),
            P(None, "tp"),
        ),
        out_specs=P("sp", "tp"),
        check_vma=False,
    )
```

profile of v0, /device:TPU:513, one launch (start us, length us, event | category | flops | bytes accessed | tf_op | source)
XLA Modules:
  0.0 175.0 jit_solution(9438342788086083026)
XLA Ops:
  0.0 0.7 reshape.281
  0.7 5.6 %collective-permute-start.3 = (s32[4,32]{1,0:T(4,128)S(1)}, s32[4,32]{1,0:T(4,128)S(1)}, u32[]{:S(2)}, u32[]{:S(2)}) collective-permute-start(s32[4,32]{1,0:T(4,128)S(1)} %reshape.281), channel_id=1, source_target_pairs={{16,0},{32,16},{48,32},{64,48},{80,64},{96,80},{112,96},{128,112},... | collective-permute-start | bytes 1544 | tf_op jit(solution)/shard_map/ppermute | solution.py:41
  6.3 1.9 %collective-permute-start.2 = (s32[4,32]{1,0:T(4,128)S(1)}, s32[4,32]{1,0:T(4,128)S(1)}, u32[]{:S(2)}, u32[]{:S(2)}) collective-permute-start(s32[4,32]{1,0:T(4,128)S(1)} %reshape.281), channel_id=1, source_target_pairs={{0,16},{16,32},{32,48},{48,64},{64,80},{80,96},{96,112},{112,128},... | collective-permute-start | bytes 1544 | tf_op jit(solution)/shard_map/ppermute | solution.py:38
  8.2 0.9 copy.58
  9.1 0.9 broadcast_in_dim.50
  10.0 8.1 %all-to-all-start = ((bf16[16,128,128]{1,2,0:T(8,128)(2,1)}), bf16[16,128,128]{1,2,0:T(8,128)(2,1)S(1)}, u32[]{:S(2)}, u32[]{:S(2)}) async-start(bf16[16,128,128]{1,2,0:T(8,128)(2,1)} %broadcast_in_dim.50), calls=%async_computation | async-start | bytes 1048576 | tf_op jit(solution)/shard_map/all_to_all | solution.py:24
  19.0 1.4 convolution_bitcast_fusion.1
  21.2 0.6 copy.64
  22.8 12.5 %all-to-all-done = bf16[16,128,128]{1,2,0:T(8,128)(2,1)S(1)} async-done(((bf16[16,128,128]{1,2,0:T(8,128)(2,1)}), bf16[16,128,128]{1,2,0:T(8,128)(2,1)S(1)}, u32[]{:S(2)}, u32[]{:S(2)}) %all-to-all-start) | async-done | bytes 524320 | tf_op jit(solution)/shard_map/all_to_all | solution.py:24
  35.7 0.9 copy-done.3
  36.9 7.0 %collective-permute-start.5 = (bf16[4,32,128]{2,1,0:T(8,128)(2,1)S(1)}, bf16[4,32,128]{2,1,0:T(8,128)(2,1)S(1)}, u32[]{:S(2)}, u32[]{:S(2)}) collective-permute-start(bf16[4,32,128]{2,1,0:T(8,128)(2,1)S(1)} %bitcast.168), channel_id=1, source_target_pairs={{16,0},{32,16},{48,32},{64,48},{80,64},{96,80},{112,96},{128,112},... | collective-permute-start | bytes 98312 | tf_op jit(solution)/shard_map/ppermute | solution.py:41
  43.8 1.9 %collective-permute-start.4 = (bf16[4,32,128]{2,1,0:T(8,128)(2,1)S(1)}, bf16[4,32,128]{2,1,0:T(8,128)(2,1)S(1)}, u32[]{:S(2)}, u32[]{:S(2)}) collective-permute-start(bf16[4,32,128]{2,1,0:T(8,128)(2,1)S(1)} %bitcast.169), channel_id=1, source_target_pairs={{0,16},{16,32},{32,48},{48,64},{64,80},{80,96},{96,112},{112,128},... | collective-permute-start | bytes 98312 | tf_op jit(solution)/shard_map/ppermute | solution.py:38
  46.1 6.7 %collective-permute-start.1 = (bf16[4,32,128]{2,1,0:T(8,128)(2,1)S(1)}, bf16[4,32,128]{2,1,0:T(8,128)(2,1)S(1)}, u32[]{:S(2)}, u32[]{:S(2)}) collective-permute-start(bf16[4,32,128]{2,1,0:T(8,128)(2,1)S(1)} %bitcast.162), channel_id=1, source_target_pairs={{16,0},{32,16},{48,32},{64,48},{80,64},{96,80},{112,96},{128,112},... | collective-permute-start | bytes 98312 | tf_op jit(solution)/shard_map/ppermute | solution.py:41
  52.8 1.9 %collective-permute-start = (bf16[4,32,128]{2,1,0:T(8,128)(2,1)S(1)}, bf16[4,32,128]{2,1,0:T(8,128)(2,1)S(1)}, u32[]{:S(2)}, u32[]{:S(2)}) collective-permute-start(bf16[4,32,128]{2,1,0:T(8,128)(2,1)S(1)} %bitcast.163), channel_id=1, source_target_pairs={{0,16},{16,32},{32,48},{48,64},{64,80},{80,96},{96,112},{112,128},... | collective-permute-start | bytes 98312 | tf_op jit(solution)/shard_map/ppermute | solution.py:38
  55.9 5.4 %collective-permute-done = bf16[4,32,128]{2,1,0:T(8,128)(2,1)S(1)} collective-permute-done((bf16[4,32,128]{2,1,0:T(8,128)(2,1)S(1)}, bf16[4,32,128]{2,1,0:T(8,128)(2,1)S(1)}, u32[]{:S(2)}, u32[]{:S(2)}) %collective-permute-start) | collective-permute-done | bytes 32800 | tf_op jit(solution)/shard_map/ppermute | solution.py:38
  64.2 21.5 %all_to_all.32 = bf16[16,128,128]{1,2,0:T(8,128)(2,1)S(1)} all-to-all(bf16[16,128,128]{1,2,0:T(8,128)(2,1)S(1)} %broadcast_in_dim.54), channel_id=1, replica_groups=mesh['sp'=48,'tp'=16] {'tp'}, dimensions={0} | all-to-all | bytes 1048576 | tf_op jit(solution)/shard_map/all_to_all | solution.py:24
  86.6 3.5 %all-to-all-start.2 = ((f32[16,1,128]{2,1,0:T(1,128)}), f32[16,1,128]{2,1,0:T(1,128)S(1)}, u32[]{:S(2)}, u32[]{:S(2)}) async-start(f32[16,1,128]{2,1,0:T(1,128)} %broadcast_in_dim.55), calls=%async_computation.2 | async-start | bytes 16384 | tf_op jit(solution)/shard_map/all_to_all | solution.py:24
  90.1 6.6 %all-to-all-done.2 = f32[16,1,128]{2,1,0:T(1,128)S(1)} async-done(((f32[16,1,128]{2,1,0:T(1,128)}), f32[16,1,128]{2,1,0:T(1,128)S(1)}, u32[]{:S(2)}, u32[]{:S(2)}) %all-to-all-start.2) | async-done | bytes 8224 | tf_op jit(solution)/shard_map/all_to_all | solution.py:24
  96.8 0.9 broadcast_in_dim.56
  97.7 4.0 %all-to-all-start.3 = ((bf16[16,128,128]{1,2,0:T(8,128)(2,1)}), bf16[16,128,128]{1,2,0:T(8,128)(2,1)S(1)}, u32[]{:S(2)}, u32[]{:S(2)}) async-start(bf16[16,128,128]{1,2,0:T(8,128)(2,1)} %broadcast_in_dim.56), calls=%async_computation.3 | async-start | bytes 1048576 | tf_op jit(solution)/shard_map/all_to_all | solution.py:24
  101.7 1.4 convolution_bitcast_fusion
  103.7 0.6 copy.73
  104.4 14.7 %all-to-all-done.3 = bf16[16,128,128]{1,2,0:T(8,128)(2,1)S(1)} async-done(((bf16[16,128,128]{1,2,0:T(8,128)(2,1)}), bf16[16,128,128]{1,2,0:T(8,128)(2,1)S(1)}, u32[]{:S(2)}, u32[]{:S(2)}) %all-to-all-start.3) | async-done | bytes 524320 | tf_op jit(solution)/shard_map/all_to_all | solution.py:24
  119.4 0.8 copy-done.4
  120.6 1.9 %collective-permute-start.9 = (bf16[4,32,128]{2,1,0:T(8,128)(2,1)S(1)}, bf16[4,32,128]{2,1,0:T(8,128)(2,1)S(1)}, u32[]{:S(2)}, u32[]{:S(2)}) collective-permute-start(bf16[4,32,128]{2,1,0:T(8,128)(2,1)S(1)} %bitcast.171), channel_id=1, source_target_pairs={{16,0},{32,16},{48,32},{64,48},{80,64},{96,80},{112,96},{128,112},... | collective-permute-start | bytes 98312 | tf_op jit(solution)/shard_map/ppermute | solution.py:41
  122.5 3.4 %collective-permute-start.8 = (bf16[4,32,128]{2,1,0:T(8,128)(2,1)S(1)}, bf16[4,32,128]{2,1,0:T(8,128)(2,1)S(1)}, u32[]{:S(2)}, u32[]{:S(2)}) collective-permute-start(bf16[4,32,128]{2,1,0:T(8,128)(2,1)S(1)} %bitcast.172), channel_id=1, source_target_pairs={{0,16},{16,32},{32,48},{48,64},{64,80},{80,96},{96,112},{112,128},... | collective-permute-start | bytes 98312 | tf_op jit(solution)/shard_map/ppermute | solution.py:38
  126.3 5.2 %collective-permute-start.7 = (bf16[4,32,128]{2,1,0:T(8,128)(2,1)S(1)}, bf16[4,32,128]{2,1,0:T(8,128)(2,1)S(1)}, u32[]{:S(2)}, u32[]{:S(2)}) collective-permute-start(bf16[4,32,128]{2,1,0:T(8,128)(2,1)S(1)} %bitcast.165), channel_id=1, source_target_pairs={{16,0},{32,16},{48,32},{64,48},{80,64},{96,80},{112,96},{128,112},... | collective-permute-start | bytes 98312 | tf_op jit(solution)/shard_map/ppermute | solution.py:41
  131.5 2.1 %collective-permute-start.6 = (bf16[4,32,128]{2,1,0:T(8,128)(2,1)S(1)}, bf16[4,32,128]{2,1,0:T(8,128)(2,1)S(1)}, u32[]{:S(2)}, u32[]{:S(2)}) collective-permute-start(bf16[4,32,128]{2,1,0:T(8,128)(2,1)S(1)} %bitcast.166), channel_id=1, source_target_pairs={{0,16},{16,32},{32,48},{48,64},{64,80},{80,96},{96,112},{112,128},... | collective-permute-start | bytes 98312 | tf_op jit(solution)/shard_map/ppermute | solution.py:38
  134.8 5.0 %collective-permute-done.6 = bf16[4,32,128]{2,1,0:T(8,128)(2,1)S(1)} collective-permute-done((bf16[4,32,128]{2,1,0:T(8,128)(2,1)S(1)}, bf16[4,32,128]{2,1,0:T(8,128)(2,1)S(1)}, u32[]{:S(2)}, u32[]{:S(2)}) %collective-permute-start.6) | collective-permute-done | bytes 32800 | tf_op jit(solution)/shard_map/ppermute | solution.py:38
  142.6 21.3 %all_to_all.33 = bf16[16,128,128]{1,2,0:T(8,128)(2,1)S(1)} all-to-all(bf16[16,128,128]{1,2,0:T(8,128)(2,1)S(1)} %broadcast_in_dim.58), channel_id=1, replica_groups=mesh['sp'=48,'tp'=16] {'tp'}, dimensions={0} | all-to-all | bytes 1048576 | tf_op jit(solution)/shard_map/all_to_all | solution.py:24
  164.4 9.8 %all_to_all.34 = f32[16,1,128]{2,1,0:T(1,128)S(1)} all-to-all(f32[16,1,128]{2,1,0:T(1,128)S(1)} %broadcast_in_dim.59), channel_id=1, replica_groups=mesh['sp'=48,'tp'=16] {'tp'}, dimensions={0} | all-to-all | bytes 16384 | tf_op jit(solution)/shard_map/all_to_all | solution.py:24
  174.3 0.7 copy.79
  (102 shorter events, 14.5 us)
Async XLA Ops:
  0.7 21.1 %collective-permute-start.3 = (s32[4,32]{1,0:T(4,128)S(1)}, s32[4,32]{1,0:T(4,128)S(1)}, u32[]{:S(2)}, u32[]{:S(2)}) collective-permute-start(s32[4,32]{1,0:T(4,128)S(1)} %reshape.281), channel_id=1, source_target_pairs={{16,0},{32,16},{48,32},{64,48},{80,64},{96,80},{112,96},{128,112},... | collective-permute-start | bytes 1544 | tf_op jit(solution)/shard_map/ppermute | solution.py:41
  6.3 15.6 %collective-permute-start.2 = (s32[4,32]{1,0:T(4,128)S(1)}, s32[4,32]{1,0:T(4,128)S(1)}, u32[]{:S(2)}, u32[]{:S(2)}) collective-permute-start(s32[4,32]{1,0:T(4,128)S(1)} %reshape.281), channel_id=1, source_target_pairs={{0,16},{16,32},{32,48},{48,64},{64,80},{80,96},{96,112},{112,128},... | collective-permute-start | bytes 1544 | tf_op jit(solution)/shard_map/ppermute | solution.py:38
  10.0 25.3 %all-to-all-start = ((bf16[16,128,128]{1,2,0:T(8,128)(2,1)}), bf16[16,128,128]{1,2,0:T(8,128)(2,1)S(1)}, u32[]{:S(2)}, u32[]{:S(2)}) async-start(bf16[16,128,128]{1,2,0:T(8,128)(2,1)} %broadcast_in_dim.50), calls=%async_computation | async-start | bytes 1048576 | tf_op jit(solution)/shard_map/all_to_all | solution.py:24
  18.1 0.7 copy-start.1
  18.1 0.8 copy-start
  35.3 1.2 copy-start.3
  35.3 10.5 %copy-start.5 = (bf16[2,2048,128]{2,1,0:T(8,128)(2,1)S(1)}, bf16[2,2048,128]{2,1,0:T(8,128)(2,1)}, u32[]{:S(2)}) copy-start(bf16[2,2048,128]{2,1,0:T(8,128)(2,1)} %param.18) | copy-start | bytes 3145732
  36.5 18.2 %copy-start.7 = (bf16[2,2048,128]{2,1,0:T(8,128)(2,1)S(1)}, bf16[2,2048,128]{2,1,0:T(8,128)(2,1)}, u32[]{:S(2)}) copy-start(bf16[2,2048,128]{2,1,0:T(8,128)(2,1)} %param.16) | copy-start | bytes 3145732
  36.9 18.3 %collective-permute-start.5 = (bf16[4,32,128]{2,1,0:T(8,128)(2,1)S(1)}, bf16[4,32,128]{2,1,0:T(8,128)(2,1)S(1)}, u32[]{:S(2)}, u32[]{:S(2)}) collective-permute-start(bf16[4,32,128]{2,1,0:T(8,128)(2,1)S(1)} %bitcast.168), channel_id=1, source_target_pairs={{16,0},{32,16},{48,32},{64,48},{80,64},{96,80},{112,96},{128,112},... | collective-permute-start | bytes 98312 | tf_op jit(solution)/shard_map/ppermute | solution.py:41
  43.8 11.4 %collective-permute-start.4 = (bf16[4,32,128]{2,1,0:T(8,128)(2,1)S(1)}, bf16[4,32,128]{2,1,0:T(8,128)(2,1)S(1)}, u32[]{:S(2)}, u32[]{:S(2)}) collective-permute-start(bf16[4,32,128]{2,1,0:T(8,128)(2,1)S(1)} %bitcast.169), channel_id=1, source_target_pairs={{0,16},{16,32},{32,48},{48,64},{64,80},{80,96},{96,112},{112,128},... | collective-permute-start | bytes 98312 | tf_op jit(solution)/shard_map/ppermute | solution.py:38
  46.1 9.7 %collective-permute-start.1 = (bf16[4,32,128]{2,1,0:T(8,128)(2,1)S(1)}, bf16[4,32,128]{2,1,0:T(8,128)(2,1)S(1)}, u32[]{:S(2)}, u32[]{:S(2)}) collective-permute-start(bf16[4,32,128]{2,1,0:T(8,128)(2,1)S(1)} %bitcast.162), channel_id=1, source_target_pairs={{16,0},{32,16},{48,32},{64,48},{80,64},{96,80},{112,96},{128,112},... | collective-permute-start | bytes 98312 | tf_op jit(solution)/shard_map/ppermute | solution.py:41
  52.8 8.5 %collective-permute-start = (bf16[4,32,128]{2,1,0:T(8,128)(2,1)S(1)}, bf16[4,32,128]{2,1,0:T(8,128)(2,1)S(1)}, u32[]{:S(2)}, u32[]{:S(2)}) collective-permute-start(bf16[4,32,128]{2,1,0:T(8,128)(2,1)S(1)} %bitcast.163), channel_id=1, source_target_pairs={{0,16},{16,32},{32,48},{48,64},{64,80},{80,96},{96,112},{112,128},... | collective-permute-start | bytes 98312 | tf_op jit(solution)/shard_map/ppermute | solution.py:38
  63.8 21.9 %copy-start.9 = (bf16[2,2048,128]{2,1,0:T(8,128)(2,1)S(1)}, bf16[2,2048,128]{2,1,0:T(8,128)(2,1)}, u32[]{:S(2)}) copy-start(bf16[2,2048,128]{2,1,0:T(8,128)(2,1)} %param.20) | copy-start | bytes 3145732
  86.6 3.5 %copy-start.2 = (f32[2,128]{1,0:T(2,128)S(1)}, f32[2,128]{1,0:T(2,128)}, u32[]{:S(2)}) copy-start(f32[2,128]{1,0:T(2,128)} %param.21) | copy-start | bytes 3076
  86.6 10.1 %all-to-all-start.2 = ((f32[16,1,128]{2,1,0:T(1,128)}), f32[16,1,128]{2,1,0:T(1,128)S(1)}, u32[]{:S(2)}, u32[]{:S(2)}) async-start(f32[16,1,128]{2,1,0:T(1,128)} %broadcast_in_dim.55), calls=%async_computation.2 | async-start | bytes 16384 | tf_op jit(solution)/shard_map/all_to_all | solution.py:24
  97.7 21.3 %all-to-all-start.3 = ((bf16[16,128,128]{1,2,0:T(8,128)(2,1)}), bf16[16,128,128]{1,2,0:T(8,128)(2,1)S(1)}, u32[]{:S(2)}, u32[]{:S(2)}) async-start(bf16[16,128,128]{1,2,0:T(8,128)(2,1)} %broadcast_in_dim.56), calls=%async_computation.3 | async-start | bytes 1048576 | tf_op jit(solution)/shard_map/all_to_all | solution.py:24
  119.0 1.2 copy-start.4
  119.0 6.9 %copy-start.6 = (bf16[2,2048,128]{2,1,0:T(8,128)(2,1)S(1)}, bf16[2,2048,128]{2,1,0:T(8,128)(2,1)}, u32[]{:S(2)}) copy-start(bf16[2,2048,128]{2,1,0:T(8,128)(2,1)} %param.18) | copy-start | bytes 3145732
  120.3 13.4 %copy-start.8 = (bf16[2,2048,128]{2,1,0:T(8,128)(2,1)S(1)}, bf16[2,2048,128]{2,1,0:T(8,128)(2,1)}, u32[]{:S(2)}) copy-start(bf16[2,2048,128]{2,1,0:T(8,128)(2,1)} %param.16) | copy-start | bytes 3145732
  120.6 13.5 %collective-permute-start.9 = (bf16[4,32,128]{2,1,0:T(8,128)(2,1)S(1)}, bf16[4,32,128]{2,1,0:T(8,128)(2,1)S(1)}, u32[]{:S(2)}, u32[]{:S(2)}) collective-permute-start(bf16[4,32,128]{2,1,0:T(8,128)(2,1)S(1)} %bitcast.171), channel_id=1, source_target_pairs={{16,0},{32,16},{48,32},{64,48},{80,64},{96,80},{112,96},{128,112},... | collective-permute-start | bytes 98312 | tf_op jit(solution)/shard_map/ppermute | solution.py:41
  122.5 11.6 %collective-permute-start.8 = (bf16[4,32,128]{2,1,0:T(8,128)(2,1)S(1)}, bf16[4,32,128]{2,1,0:T(8,128)(2,1)S(1)}, u32[]{:S(2)}, u32[]{:S(2)}) collective-permute-start(bf16[4,32,128]{2,1,0:T(8,128)(2,1)S(1)} %bitcast.172), channel_id=1, source_target_pairs={{0,16},{16,32},{32,48},{48,64},{64,80},{80,96},{96,112},{112,128},... | collective-permute-start | bytes 98312 | tf_op jit(solution)/shard_map/ppermute | solution.py:38
  126.3 8.5 %collective-permute-start.7 = (bf16[4,32,128]{2,1,0:T(8,128)(2,1)S(1)}, bf16[4,32,128]{2,1,0:T(8,128)(2,1)S(1)}, u32[]{:S(2)}, u32[]{:S(2)}) collective-permute-start(bf16[4,32,128]{2,1,0:T(8,128)(2,1)S(1)} %bitcast.165), channel_id=1, source_target_pairs={{16,0},{32,16},{48,32},{64,48},{80,64},{96,80},{112,96},{128,112},... | collective-permute-start | bytes 98312 | tf_op jit(solution)/shard_map/ppermute | solution.py:41
  131.5 8.3 %collective-permute-start.6 = (bf16[4,32,128]{2,1,0:T(8,128)(2,1)S(1)}, bf16[4,32,128]{2,1,0:T(8,128)(2,1)S(1)}, u32[]{:S(2)}, u32[]{:S(2)}) collective-permute-start(bf16[4,32,128]{2,1,0:T(8,128)(2,1)S(1)} %bitcast.166), channel_id=1, source_target_pairs={{0,16},{16,32},{32,48},{48,64},{64,80},{80,96},{96,112},{112,128},... | collective-permute-start | bytes 98312 | tf_op jit(solution)/shard_map/ppermute | solution.py:38
  142.2 21.8 %copy-start.10 = (bf16[2,2048,128]{2,1,0:T(8,128)(2,1)S(1)}, bf16[2,2048,128]{2,1,0:T(8,128)(2,1)}, u32[]{:S(2)}) copy-start(bf16[2,2048,128]{2,1,0:T(8,128)(2,1)} %param.20) | copy-start | bytes 3145732
where the time goes:
time: 176 us; the launch traced here: 175 us
  starting transfers between devices  53.2 us (30%)
  blocking collectives  52.6 us (30%)
  waiting for transfers between devices  44.2 us (25%)
  local copies, waits for them, and re-layouts  13.5 us (8%)
  matrix products  8.04 us (5%)
  other arithmetic  2.84 us (2%)
    all_to_all x3, blocking collectives, from_everyone(): lax.all_to_all(jnp.broadcast_to(array[None], (length, *array.shape)), axi...  52.6 us
    all_to_all x3, waiting for transfers between devices, from_everyone(): lax.all_to_all(jnp.broadcast_to(array[None], (length, *array.shape)), axi...  33.7 us
    ppermute x5, starting transfers between devices, extended(): lax.ppermute(lax.slice_in_dim(block, 0, width, axis=dim), axis, backward)  26.4 us
    all_to_all x3, starting transfers between devices, from_everyone(): lax.all_to_all(jnp.broadcast_to(array[None], (length, *array.shape)), axi...  15.6 us
    ppermute x5, starting transfers between devices, extended(): lax.ppermute(lax.slice_in_dim(block, block.shape[dim] - width, None, axis...  11.2 us
    ppermute x5, waiting for transfers between devices, extended(): lax.ppermute(lax.slice_in_dim(block, block.shape[dim] - width, None, axis...  10.5 us
    dot_general x4, matrix products, shards(): jnp.einsum('hrt,ijr,ckt->ihcjk', offset_bias[layer_index], row_onehot, co...  3.99 us
  transfers between devices with their start and end apart: 13, of which 5 were waited for; matrix products, arithmetic and copies ran while one was open for 6% of the time, Pallas kernels for 0%

commit v1 on v0

v1 whole, which is shorter than its diff:
```python
import functools

import jax
import jax.numpy as jnp
from jax import lax
from jax.experimental import pallas as pl
from jax.experimental.pallas import tpu as pltpu
from jax.sharding import PartitionSpec as P

HEAD_DIM = 64
WIN_ROWS = 8
WIN_COLS = 16
GRID_W = 32
LAYERS = 2
EPSILON = 1e-06
RIM = WIN_ROWS // 2
BIAS_ROWS = 2 * WIN_ROWS
LOWEST = -1e30

VMEM = pl.BlockSpec(memory_space=pltpu.VMEM)
SMEM = pl.BlockSpec(memory_space=pltpu.SMEM)


def call(body, outs, specs, name):
    return pl.pallas_call(
        body,
        out_shape=outs,
        in_specs=specs,
        out_specs=jax.tree.map(lambda _: VMEM, outs),
        name=name,
    )


def struct(shape, dtype):
    return jax.ShapeDtypeStruct(shape, dtype)


def joined(ref, rows):
    return jnp.concatenate([ref[i, :rows] for i in range(ref.shape[0])], axis=1)


def as_column(row, size):
    return jnp.transpose(jnp.broadcast_to(row, (size, size)))


def heads_from(wide, gain, weights, q_ref, kv_ref):
    tokens, model_width = wide.shape
    cols = weights[0].shape[1]
    scaler = lax.rsqrt(jnp.sum(wide * wide, axis=1, keepdims=True) / model_width + EPSILON)
    scaled = (wide * gain).astype(jnp.bfloat16)
    query, key, value = (
        (jnp.dot(scaled, w, preferred_element_type=jnp.float32) * scaler).astype(jnp.bfloat16)
        for w in weights
    )
    q_ref[...] = query
    kv_ref[:tokens, :cols] = key
    kv_ref[:tokens, cols:] = value


def first_heads(x_ref, gain_ref, docs_ref, wq_ref, wk_ref, wv_ref, q_ref, kv_ref):
    tokens = x_ref.shape[1]
    wide = joined(x_ref, tokens).astype(jnp.float32)
    heads_from(wide, gain_ref[0:1], (wq_ref[0], wk_ref[0], wv_ref[0]), q_ref, kv_ref)
    pad = kv_ref.shape[0] - tokens
    row = docs_ref[...].astype(jnp.float32)
    row = jnp.concatenate([row] * (kv_ref.shape[1] // tokens), axis=1)
    kv_ref[tokens:] = jnp.broadcast_to(row, (pad, kv_ref.shape[1])).astype(jnp.bfloat16)


def next_heads(at_ref, x_ref, b_ref, gain_ref, own_gain_ref, wq_ref, wk_ref, wv_ref, q_ref, kv_ref, own_ref):
    tokens = x_ref.shape[1]
    count = x_ref.shape[0]
    branch = joined(b_ref, tokens).astype(jnp.float32)
    scale = lax.rsqrt(jnp.sum(branch * branch, axis=1, keepdims=True) / branch.shape[1] + EPSILON)
    parts = jnp.concatenate([b_ref[i, tokens:] for i in range(count)], axis=1).astype(jnp.float32)
    post = parts[0:1] + parts[1:2] + parts[2:3]
    stream = joined(x_ref, tokens).astype(jnp.float32)
    stream = (stream + branch * scale * post).astype(jnp.bfloat16)
    heads_from(
        stream.astype(jnp.float32), gain_ref[1:2], (wq_ref[1], wk_ref[1], wv_ref[1]), q_ref, kv_ref
    )
    at = at_ref[0]
    own = x_ref[at].astype(jnp.float32)
    own_branch = b_ref[at][:tokens].astype(jnp.float32)
    own_ref[...] = (own + own_branch * scale * own_gain_ref[0:1]).astype(jnp.bfloat16)


def attend(layer, last_row, at_ref, q_ref, own_ref, low_ref, high_ref, dl_ref, do_ref, dh_ref, bias_ref, out_ref):
    tokens, cols = q_ref.shape
    rows = tokens // GRID_W
    keys = 3 * tokens
    first_row = at_ref[1] * rows
    blocks = (low_ref, own_ref, high_ref)
    key = jnp.concatenate([b[:tokens, :cols] for b in blocks], axis=0)
    value = jnp.concatenate([b[:tokens, cols:] for b in blocks], axis=0)
    key_docs = jnp.concatenate([d[:1, :tokens].astype(jnp.float32) for d in (dl_ref, do_ref, dh_ref)], axis=1)
    query_docs = as_column(do_ref[:1, :tokens].astype(jnp.float32), tokens)
    query_docs = jnp.concatenate([query_docs] * 3, axis=1)
    token = lax.broadcasted_iota(jnp.int32, (tokens, keys), 0)
    other = lax.broadcasted_iota(jnp.int32, (tokens, keys), 1)
    row, col = first_row + token // GRID_W, token % GRID_W
    key_row, key_col = first_row - rows + other // GRID_W, other % GRID_W
    row_start = jnp.clip(row - RIM, 0, last_row - WIN_ROWS)
    col_start = jnp.clip(col - WIN_COLS // 2, 0, GRID_W - WIN_COLS)
    allowed = (
        (key_row >= row_start)
        & (key_row < row_start + WIN_ROWS)
        & (key_col >= col_start)
        & (key_col < col_start + WIN_COLS)
        & (key_docs == query_docs)
    )
    query = q_ref[...]
    lane = lax.broadcasted_iota(jnp.int32, (tokens, cols), 1)
    result = jnp.zeros((tokens, cols), jnp.float32)
    for head in range(cols // HEAD_DIM):
        mine = (lane >= head * HEAD_DIM) & (lane < (head + 1) * HEAD_DIM)
        flat = jnp.broadcast_to(bias_ref[layer, head : head + 1], (GRID_W, bias_ref.shape[2]))
        width = flat.shape[1]
        bias = jnp.concatenate(
            [
                pltpu.roll(
                    flat,
                    (-(WIN_COLS - 1) - (WIN_ROWS - 1 - rows - r) * GRID_W) % width,
                    1,
                    stride=1,
                    stride_axis=0,
                )[:, :keys]
                for r in range(rows)
            ],
            axis=0,
        )
        scores = lax.dot_general(
            jnp.where(mine, query, jnp.zeros_like(query)),
            key,
            (((1,), (1,)), ((), ())),
            preferred_element_type=jnp.float32,
        )
        scores = jnp.where(allowed, scores * HEAD_DIM ** (-0.5) + bias, LOWEST)
        lifted = jnp.exp(scores - jnp.max(scores, axis=1, keepdims=True))
        weights = (lifted / jnp.sum(lifted, axis=1, keepdims=True)).astype(jnp.bfloat16)
        summed = jnp.dot(weights, value, preferred_element_type=jnp.float32)
        result = jnp.where(mine, summed, result)
    out_ref[...] = result.astype(jnp.bfloat16)


def first_out(a_ref, w_ref, post_ref, out_ref):
    tokens = a_ref.shape[1]
    branch = jnp.dot(joined(a_ref, tokens), w_ref[0], preferred_element_type=jnp.float32)
    out_ref[:tokens] = branch.astype(jnp.bfloat16)
    post = post_ref[0:1]
    high = post.astype(jnp.bfloat16)
    rest = post - high.astype(jnp.float32)
    middle = rest.astype(jnp.bfloat16)
    low = (rest - middle.astype(jnp.float32)).astype(jnp.bfloat16)
    pad = out_ref.shape[0] - tokens
    place = lax.broadcasted_iota(jnp.int32, (pad, post.shape[1]), 0)
    rows = jnp.where(
        place == 0,
        high.astype(jnp.float32),
        jnp.where(place == 1, middle.astype(jnp.float32), low.astype(jnp.float32)),
    )
    out_ref[tokens:] = rows.astype(jnp.bfloat16)


def last_out(a_ref, w_ref, branch_ref, squares_ref):
    tokens = a_ref.shape[1]
    branch = jnp.dot(joined(a_ref, tokens), w_ref[1], preferred_element_type=jnp.float32)
    branch_ref[...] = branch
    squares = jnp.sum(jnp.transpose(branch * branch), axis=0, keepdims=True)
    squares_ref[...] = jnp.broadcast_to(squares[None], squares_ref.shape)


def finish(model_width, squares_ref, branch_ref, own_ref, post_ref, out_ref):
    tokens = branch_ref.shape[0]
    total = jnp.sum(squares_ref[...], axis=0)
    scale = as_column(lax.rsqrt(total / model_width + EPSILON), tokens)
    out_ref[...] = (
        own_ref[...].astype(jnp.float32) + branch_ref[...] * scale * post_ref[1:2]
    ).astype(jnp.bfloat16)


def neighbours(block):
    count = lax.axis_size("sp")
    forward = [(i, i + 1) for i in range(count - 1)]
    backward = [(i + 1, i) for i in range(count - 1)]
    return lax.ppermute(block, "sp", forward), lax.ppermute(block, "sp", backward)


def shards(
    grid_in,
    documents,
    pre_gain,
    query_weight,
    key_weight,
    value_weight,
    offset_bias,
    out_weight,
    post_gain,
):
    tokens, feat = grid_in.shape
    model_width = pre_gain.shape[1]
    cols = query_weight.shape[2]
    heads = offset_bias.shape[1]
    bf16, f32 = jnp.bfloat16, jnp.float32
    members = lax.axis_size("tp")
    all_rows = tokens // GRID_W * lax.axis_size("sp")
    pad = 16
    at = jnp.stack([lax.axis_index("tp"), lax.axis_index("sp")]).astype(jnp.int32)
    docs = documents.reshape(1, tokens)
    bias = jnp.pad(
        offset_bias, ((0, 0), (0, 0), (0, BIAS_ROWS - 2 * WIN_ROWS + 1), (0, GRID_W - 2 * WIN_COLS + 1))
    ).reshape(LAYERS, heads, BIAS_ROWS * GRID_W)

    stream = lax.all_gather(grid_in, "tp", axis=0)
    query, kv = call(
        first_heads,
        (struct((tokens, cols), bf16), struct((tokens + pad, 2 * cols), bf16)),
        [VMEM] * 6,
        "first_heads",
    )(stream, pre_gain, docs, query_weight, key_weight, value_weight)
    low, high = neighbours(kv)
    doc_rows = (low[tokens:], kv[tokens:], high[tokens:])

    def attention(layer, query, kv, low, high):
        return call(
            functools.partial(attend, layer, all_rows),
            struct((tokens, cols), bf16),
            [SMEM] + [VMEM] * 8,
            "attend%d" % layer,
        )(at, query, kv, low, high, *doc_rows, bias)

    attended = lax.all_gather(attention(0, query, kv, low, high), "tp", axis=0)
    branch = call(first_out, struct((tokens + pad, feat), bf16), [VMEM] * 3, "first_out")(
        attended, out_weight, post_gain
    )
    branch = lax.all_gather(branch, "tp", axis=0)
    query, kv, own = call(
        next_heads,
        (
            struct((tokens, cols), bf16),
            struct((tokens, 2 * cols), bf16),
            struct((tokens, feat), bf16),
        ),
        [SMEM] + [VMEM] * 7,
        "next_heads",
    )(at, stream, branch, pre_gain, post_gain, query_weight, key_weight, value_weight)
    low, high = neighbours(kv)
    attended = lax.all_gather(attention(1, query, kv, low, high), "tp", axis=0)
    branch, squares = call(
        last_out,
        (struct((tokens, feat), f32), struct((members, 1, tokens), f32)),
        [VMEM] * 2,
        "last_out",
    )(attended, out_weight)
    squares = lax.all_to_all(squares, "tp", 0, 0, tiled=True)
    return call(
        functools.partial(finish, model_width), struct((tokens, feat), bf16), [VMEM] * 4, "finish"
    )(squares, branch, own, post_gain)


def solution(mesh):
    return jax.shard_map(
        shards,
        mesh=mesh,
        in_specs=(
            P("sp", "tp"),
            P("sp"),
            P(),
            P(None, None, "tp"),
            P(None, None, "tp"),
            P(None, None, "tp"),
            P(None, "tp", None, None),
            P(None, None, "tp"),
            P(None, "tp"),
        ),
        out_specs=P("sp", "tp"),
        check_vma=False,
    )
```

time: 176 us -> 136 us (0.77)
  starting transfers between devices: 53.2 us -> 12.8 us
  blocking collectives: 52.6 us -> 90.4 us
  waiting for transfers between devices: 44.2 us -> 9.07 us
  Pallas kernels: 0 us -> 18.1 us
  local copies, waits for them, and re-layouts: 13.5 us -> 3.87 us
  matrix products: 8.04 us -> 0 us
  other arithmetic: 2.84 us -> 0.6 us
    all_gather x0 -> x4, blocking collectives: none -> 78.5 us  [the longest x1 21.2 us: shards(): stream = lax.all_gather(grid_in, 'tp', axis=0)]
    all_to_all x3 -> x1, blocking collectives: 52.6 us -> 11.9 us  [shards(): squares = lax.all_to_all(squares, 'tp', 0, 0, tiled=True)]
    all_to_all x3 -> x0, waiting for transfers between devices: 33.7 us -> none  [from_everyone(): lax.all_to_all(jnp.broadcast_to(array[None], (length, *array.shape)), axi...]
    ppermute x10 -> x4, starting transfers between devices: 37.6 us -> 12.8 us  [the longest x2 7.9 us: neighbours(): lax.ppermute(block, 'sp', backward)]
    pallas_call x0 -> x7, Pallas kernels: none -> 18.1 us  [the longest x2 4.97 us: attention(): call(functools.partial(attend, layer, all_rows), struct((tokens, cols), b...]
    all_to_all x3 -> x0, starting transfers between devices: 15.6 us -> none  [from_everyone(): lax.all_to_all(jnp.broadcast_to(array[None], (length, *array.shape)), axi...]
    dot_general x14 -> x0, matrix products: 7.49 us -> none  [the longest x4 3.99 us: shards(): jnp.einsum('hrt,ijr,ckt->ihcjk', offset_bias[layer_index], row_onehot, co...]
    broadcast_in_dim x11 -> x0, local copies, waits for them, and re-layouts: 3.13 us -> none  [the longest x10 3.05 us: from_everyone(): jnp.broadcast_to(array[None], (length, *array.shape))]
  transfers between devices with their start and end apart: 13 -> 4, of which waited for: 5 -> 3; matrix products, arithmetic and copies ran while one was open for 6% -> 2% of each run, Pallas kernels for 0% -> 0%
where the time goes in v1:
time: 136 us; the launch traced here: 135 us
  blocking collectives  90.4 us (66%)
  Pallas kernels  18.1 us (13%)
  starting transfers between devices  12.8 us (9%)
  waiting for transfers between devices  9.07 us (7%)
  local copies, waits for them, and re-layouts  3.87 us (3%)
    all_gather x1, blocking collectives, shards(): stream = lax.all_gather(grid_in, 'tp', axis=0)  21.2 us
    all_gather x1, blocking collectives, shards(): attended = lax.all_gather(attention(1, query, kv, low, high), 'tp', axis=0)  19.4 us
    all_gather x1, blocking collectives, shards(): attended = lax.all_gather(attention(0, query, kv, low, high), 'tp', axis=0)  19.4 us
    all_gather x1, blocking collectives, shards(): branch = lax.all_gather(branch, 'tp', axis=0)  18.6 us
    all_to_all x1, blocking collectives, shards(): squares = lax.all_to_all(squares, 'tp', 0, 0, tiled=True)  11.9 us
    ppermute x2, waiting for transfers between devices, neighbours(): lax.ppermute(block, 'sp', forward)  8.77 us
    ppermute x2, starting transfers between devices, neighbours(): lax.ppermute(block, 'sp', backward)  7.9 us
    pallas_call x2, Pallas kernels, attention(): call(functools.partial(attend, layer, all_rows), struct((tokens, cols), b...  4.97 us
  transfers between devices with their start and end apart: 4, of which 3 were waited for; matrix products, arithmetic and copies ran while one was open for 2% of the time, Pallas kernels for 0%

profile of v1, /device:TPU:513, one launch (start us, length us, event | category | flops | bytes accessed | tf_op | source)
XLA Modules:
  0.0 134.9 jit_solution(11165980650338733978)
XLA Ops:
  0.0 21.2 %all-gather = bf16[2048,128]{1,0:T(8,128)(2,1)} all-gather(bf16[128,128]{1,0:T(8,128)(2,1)} %param.9), channel_id=2, replica_groups=mesh['sp'=48,'tp'=16] {'tp'}, dimensions={0}, use_global_device_ids=true | all-gather | bytes 557056 | tf_op jit(solution)/shard_map/all_gather | solution.py:214
  21.2 0.0 copy-start.4
  21.2 3.3 %first_heads.1 = (bf16[128,128]{1,0:T(8,128)(2,1)}, bf16[144,256]{1,0:T(8,128)(2,1)}) custom-call(bf16[16,128,128]{2,1,0:T(8,128)(2,1)} %bitcast.9, f32[2,2048]{1,0:T(2,128)} %gain_ref.3, s32[1,128]{1,0:T(1,128)} %bitcast.14, bf16[2,2048,128]{2,1,0:T(8,128)(2,1)} %wq_ref.3, bf16[2,2048,128]{2,1,0:T(8,128)(2,1)} %wk_ref.3, bf16[2,2048,128]{2,1,0:T(8,128)(2,1)} %wv_ref.3), custom_call_target="tpu_custom_call" | custom-call | tf_op jit(solution)/shard_map/first_heads/pallas_call | solution.py:215
  24.4 5.6 %collective-permute-start.1 = (bf16[144,256]{1,0:T(8,128)(2,1)}, bf16[144,256]{1,0:T(8,128)(2,1)S(1)}, u32[]{:S(2)}, u32[]{:S(2)}) collective-permute-start(bf16[144,256]{1,0:T(8,128)(2,1)} %get-tuple-element.13.own_ref), channel_id=1, source_target_pairs={{16,0},{32,16},{48,32},{64,48},{80,64},{96,80},{112,96},{128,112},... | collective-permute-start | bytes 221192 | tf_op jit(solution)/shard_map/ppermute | solution.py:186
  30.0 1.9 %collective-permute-start = (bf16[144,256]{1,0:T(8,128)(2,1)}, bf16[144,256]{1,0:T(8,128)(2,1)S(1)}, u32[]{:S(2)}, u32[]{:S(2)}) collective-permute-start(bf16[144,256]{1,0:T(8,128)(2,1)} %get-tuple-element.13.own_ref), channel_id=1, source_target_pairs={{0,16},{16,32},{32,48},{48,64},{64,80},{80,96},{96,112},{112,128},... | collective-permute-start | bytes 221192 | tf_op jit(solution)/shard_map/ppermute | solution.py:186
  31.9 1.3 slice.10.do_ref
  33.2 0.0 copy-done.4
  33.3 0.7 reshape.7.bias_ref
  33.9 0.6 pad_add_fusion.at_ref
  34.5 0.0 collective-permute-done.1.high_ref
  34.5 0.0 copy-start
  34.5 0.6 slice.13.dh_ref
  35.2 3.5 %collective-permute-done.low_ref = bf16[144,256]{1,0:T(8,128)(2,1)S(1)} collective-permute-done((bf16[144,256]{1,0:T(8,128)(2,1)}, bf16[144,256]{1,0:T(8,128)(2,1)S(1)}, u32[]{:S(2)}, u32[]{:S(2)}) %collective-permute-start) | collective-permute-done | bytes 73760 | tf_op jit(solution)/shard_map/ppermute | solution.py:186
  38.6 0.6 slice.12.dl_ref
  39.3 0.0 copy-done
  39.3 0.0 copy-done.1
  39.3 2.5 %attend0.1 = bf16[128,128]{1,0:T(8,128)(2,1)} custom-call(s32[2]{0:T(128)} %pad_add_fusion.at_ref, bf16[128,128]{1,0:T(8,128)(2,1)} %get-tuple-element.12.q_ref, bf16[144,256]{1,0:T(8,128)(2,1)} %get-tuple-element.13.own_ref, bf16[144,256]{1,0:T(8,128)(2,1)} %copy-done.1, bf16[144,256]{1,0:T(8,128)(2,1)} %copy-done, bf16[16,256]{1,0:T(8,128)(2,1)} %slice.12.dl_ref, ...), custom_call_target="tpu_custom_call" | custom-call | tf_op jit(solution)/shard_map/attend0/pallas_call | solution.py:225
  41.8 19.4 %all-gather.1 = bf16[2048,128]{1,0:T(8,128)(2,1)} all-gather(bf16[128,128]{1,0:T(8,128)(2,1)} %attend0.1), channel_id=3, replica_groups=mesh['sp'=48,'tp'=16] {'tp'}, dimensions={0}, use_global_device_ids=true | all-gather | bytes 557056 | tf_op jit(solution)/shard_map/all_gather | solution.py:232
  61.2 2.2 %first_out.1 = bf16[144,128]{1,0:T(8,128)(2,1)} custom-call(bf16[16,128,128]{2,1,0:T(8,128)(2,1)} %bitcast.13, bf16[2,2048,128]{2,1,0:T(8,128)(2,1)} %w_ref.3, f32[2,128]{1,0:T(2,128)} %post_ref.3), custom_call_target="tpu_custom_call" | custom-call | tf_op jit(solution)/shard_map/first_out/pallas_call | solution.py:233
  63.4 18.6 %all-gather.2 = bf16[2304,128]{1,0:T(8,128)(2,1)} all-gather(bf16[144,128]{1,0:T(8,128)(2,1)} %first_out.1), channel_id=4, replica_groups=mesh['sp'=48,'tp'=16] {'tp'}, dimensions={0}, use_global_device_ids=true | all-gather | bytes 626688 | tf_op jit(solution)/shard_map/all_gather | solution.py:236
  82.0 3.7 %next_heads.1 = (bf16[128,128]{1,0:T(8,128)(2,1)}, bf16[128,256]{1,0:T(8,128)(2,1)}, bf16[128,128]{1,0:T(8,128)(2,1)}) custom-call(s32[2]{0:T(128)} %pad_add_fusion.at_ref, bf16[16,128,128]{2,1,0:T(8,128)(2,1)} %bitcast.10, bf16[16,144,128]{2,1,0:T(8,128)(2,1)} %bitcast.11, f32[2,2048]{1,0:T(2,128)} %gain_ref.3, f32[2,128]{1,0:T(2,128)} %post_ref.3, ...), custom_call_target="tpu_custom_call" | custom-call | tf_op jit(solution)/shard_map/next_heads/pallas_call | solution.py:237
  85.7 2.3 %collective-permute-start.3 = (bf16[128,256]{1,0:T(8,128)(2,1)}, bf16[128,256]{1,0:T(8,128)(2,1)S(1)}, u32[]{:S(2)}, u32[]{:S(2)}) collective-permute-start(bf16[128,256]{1,0:T(8,128)(2,1)} %get-tuple-element.15.own_ref), channel_id=1, source_target_pairs={{16,0},{32,16},{48,32},{64,48},{80,64},{96,80},{112,96},{128,112},... | collective-permute-start | bytes 196616 | tf_op jit(solution)/shard_map/ppermute | solution.py:186
  88.0 2.9 %collective-permute-start.2 = (bf16[128,256]{1,0:T(8,128)(2,1)}, bf16[128,256]{1,0:T(8,128)(2,1)S(1)}, u32[]{:S(2)}, u32[]{:S(2)}) collective-permute-start(bf16[128,256]{1,0:T(8,128)(2,1)} %get-tuple-element.15.own_ref), channel_id=1, source_target_pairs={{0,16},{16,32},{32,48},{48,64},{64,80},{80,96},{96,112},{112,128},... | collective-permute-start | bytes 196616 | tf_op jit(solution)/shard_map/ppermute | solution.py:186
  91.0 0.3 collective-permute-done.3.high_ref
  91.3 5.3 %collective-permute-done.2.low_ref = bf16[128,256]{1,0:T(8,128)(2,1)S(1)} collective-permute-done((bf16[128,256]{1,0:T(8,128)(2,1)}, bf16[128,256]{1,0:T(8,128)(2,1)S(1)}, u32[]{:S(2)}, u32[]{:S(2)}) %collective-permute-start.2) | collective-permute-done | bytes 65568 | tf_op jit(solution)/shard_map/ppermute | solution.py:186
  96.6 0.0 copy-done.2
  96.6 0.6 copy-done.3
  97.2 2.5 %attend1.1 = bf16[128,128]{1,0:T(8,128)(2,1)} custom-call(s32[2]{0:T(128)} %pad_add_fusion.at_ref, bf16[128,128]{1,0:T(8,128)(2,1)} %get-tuple-element.14.q_ref, bf16[128,256]{1,0:T(8,128)(2,1)} %get-tuple-element.15.own_ref, bf16[128,256]{1,0:T(8,128)(2,1)} %copy-done.3, bf16[128,256]{1,0:T(8,128)(2,1)} %copy-done.2, bf16[16,256]{1,0:T(8,128)(2,1)} %slice.12.dl_ref, ...), custom_call_target="tpu_custom_call" | custom-call | tf_op jit(solution)/shard_map/attend1/pallas_call | solution.py:225
  99.6 19.4 %all-gather.3 = bf16[2048,128]{1,0:T(8,128)(2,1)} all-gather(bf16[128,128]{1,0:T(8,128)(2,1)} %attend1.1), channel_id=5, replica_groups=mesh['sp'=48,'tp'=16] {'tp'}, dimensions={0}, use_global_device_ids=true | all-gather | bytes 557056 | tf_op jit(solution)/shard_map/all_gather | solution.py:248
  119.0 2.4 %last_out.1 = (f32[128,128]{1,0:T(8,128)}, f32[16,1,128]{2,1,0:T(1,128)}) custom-call(bf16[16,128,128]{2,1,0:T(8,128)(2,1)} %bitcast.12, bf16[2,2048,128]{2,1,0:T(8,128)(2,1)} %w_ref.3), custom_call_target="tpu_custom_call" | custom-call | tf_op jit(solution)/shard_map/last_out/pallas_call | solution.py:249
  121.4 11.9 %all_to_all.5.squares_ref = f32[16,1,128]{2,1,0:T(1,128)} all-to-all(f32[16,1,128]{2,1,0:T(1,128)} %get-tuple-element.16), channel_id=1, replica_groups=mesh['sp'=48,'tp'=16] {'tp'}, dimensions={0} | all-to-all | bytes 16384 | tf_op jit(solution)/shard_map/all_to_all | solution.py:255
  133.3 1.6 %finish.1 = bf16[128,128]{1,0:T(8,128)(2,1)} custom-call(f32[16,1,128]{2,1,0:T(1,128)} %all_to_all.5.squares_ref, f32[128,128]{1,0:T(8,128)} %get-tuple-element.17.branch_ref, bf16[128,128]{1,0:T(8,128)(2,1)} %get-tuple-element.18.own_ref, f32[2,128]{1,0:T(2,128)} %post_ref.3), custom_call_target="tpu_custom_call" | custom-call | tf_op jit(solution)/shard_map/finish/pallas_call | solution.py:256
  (5 shorter events, 0.0 us)
Async XLA Ops:
  21.2 12.1 %copy-start.4 = (f32[2,2,15,31]{3,1,2,0:T(2,128)S(1)}, f32[2,2,15,31]{3,1,2,0:T(2,128)}, u32[]{:S(2)}) copy-start(f32[2,2,15,31]{3,1,2,0:T(2,128)} %param.15) | copy-start | bytes 22324
  24.4 10.1 %collective-permute-start.1 = (bf16[144,256]{1,0:T(8,128)(2,1)}, bf16[144,256]{1,0:T(8,128)(2,1)S(1)}, u32[]{:S(2)}, u32[]{:S(2)}) collective-permute-start(bf16[144,256]{1,0:T(8,128)(2,1)} %get-tuple-element.13.own_ref), channel_id=1, source_target_pairs={{16,0},{32,16},{48,32},{64,48},{80,64},{96,80},{112,96},{128,112},... | collective-permute-start | bytes 221192 | tf_op jit(solution)/shard_map/ppermute | solution.py:186
  30.0 8.6 %collective-permute-start = (bf16[144,256]{1,0:T(8,128)(2,1)}, bf16[144,256]{1,0:T(8,128)(2,1)S(1)}, u32[]{:S(2)}, u32[]{:S(2)}) collective-permute-start(bf16[144,256]{1,0:T(8,128)(2,1)} %get-tuple-element.13.own_ref), channel_id=1, source_target_pairs={{0,16},{16,32},{32,48},{48,64},{64,80},{80,96},{96,112},{112,128},... | collective-permute-start | bytes 221192 | tf_op jit(solution)/shard_map/ppermute | solution.py:186
  34.5 4.7 %copy-start = (bf16[144,256]{1,0:T(8,128)(2,1)}, bf16[144,256]{1,0:T(8,128)(2,1)S(1)}, u32[]{:S(2)}) copy-start(bf16[144,256]{1,0:T(8,128)(2,1)S(1)} %collective-permute-done.1.high_ref) | copy-start | bytes 221188
  38.6 0.6 copy-start.1
  85.7 5.6 %collective-permute-start.3 = (bf16[128,256]{1,0:T(8,128)(2,1)}, bf16[128,256]{1,0:T(8,128)(2,1)S(1)}, u32[]{:S(2)}, u32[]{:S(2)}) collective-permute-start(bf16[128,256]{1,0:T(8,128)(2,1)} %get-tuple-element.15.own_ref), channel_id=1, source_target_pairs={{16,0},{32,16},{48,32},{64,48},{80,64},{96,80},{112,96},{128,112},... | collective-permute-start | bytes 196616 | tf_op jit(solution)/shard_map/ppermute | solution.py:186
  88.0 8.5 %collective-permute-start.2 = (bf16[128,256]{1,0:T(8,128)(2,1)}, bf16[128,256]{1,0:T(8,128)(2,1)S(1)}, u32[]{:S(2)}, u32[]{:S(2)}) collective-permute-start(bf16[128,256]{1,0:T(8,128)(2,1)} %get-tuple-element.15.own_ref), channel_id=1, source_target_pairs={{0,16},{16,32},{32,48},{48,64},{64,80},{80,96},{96,112},{112,128},... | collective-permute-start | bytes 196616 | tf_op jit(solution)/shard_map/ppermute | solution.py:186
  91.3 5.3 %copy-start.2 = (bf16[128,256]{1,0:T(8,128)(2,1)}, bf16[128,256]{1,0:T(8,128)(2,1)S(1)}, u32[]{:S(2)}) copy-start(bf16[128,256]{1,0:T(8,128)(2,1)S(1)} %collective-permute-done.3.high_ref) | copy-start | bytes 196612
  96.6 0.6 copy-start.3

commit v2 on v1

--- a/solution.py
+++ b/solution.py
@@ -22,7 +22,7 @@
 
 
 def call(body, outs, specs, name):
-    return pl.pallas_call(
+    kernel = pl.pallas_call(
         body,
         out_shape=outs,
         in_specs=specs,
@@ -30,9 +30,23 @@
         name=name,
     )
 
+    def run(*args):
+        return kernel(
+            *(
+                pltpu.with_memory_space_constraint(arg, pltpu.VMEM) if spec is VMEM else arg
+                for arg, spec in zip(args, specs, strict=True)
+            )
+        )
+
+    return run
+
 
 def struct(shape, dtype):
-    return jax.ShapeDtypeStruct(shape, dtype)
+    return pltpu.VMEM(shape, dtype)
+
+
+def of(array, layer):
+    return lax.slice_in_dim(array, layer, layer + 1, axis=0)
 
 
 def joined(ref, rows):
@@ -77,7 +91,7 @@
     stream = joined(x_ref, tokens).astype(jnp.float32)
     stream = (stream + branch * scale * post).astype(jnp.bfloat16)
     heads_from(
-        stream.astype(jnp.float32), gain_ref[1:2], (wq_ref[1], wk_ref[1], wv_ref[1]), q_ref, kv_ref
+        stream.astype(jnp.float32), gain_ref[0:1], (wq_ref[0], wk_ref[0], wv_ref[0]), q_ref, kv_ref
     )
     at = at_ref[0]
     own = x_ref[at].astype(jnp.float32)
@@ -164,7 +178,7 @@
 
 def last_out(a_ref, w_ref, branch_ref, squares_ref):
     tokens = a_ref.shape[1]
-    branch = jnp.dot(joined(a_ref, tokens), w_ref[1], preferred_element_type=jnp.float32)
+    branch = jnp.dot(joined(a_ref, tokens), w_ref[0], preferred_element_type=jnp.float32)
     branch_ref[...] = branch
     squares = jnp.sum(jnp.transpose(branch * branch), axis=0, keepdims=True)
     squares_ref[...] = jnp.broadcast_to(squares[None], squares_ref.shape)
@@ -175,7 +189,7 @@
     total = jnp.sum(squares_ref[...], axis=0)
     scale = as_column(lax.rsqrt(total / model_width + EPSILON), tokens)
     out_ref[...] = (
-        own_ref[...].astype(jnp.float32) + branch_ref[...] * scale * post_ref[1:2]
+        own_ref[...].astype(jnp.float32) + branch_ref[...] * scale * post_ref[0:1]
     ).astype(jnp.bfloat16)
 
 
@@ -217,7 +231,7 @@
         (struct((tokens, cols), bf16), struct((tokens + pad, 2 * cols), bf16)),
         [VMEM] * 6,
         "first_heads",
-    )(stream, pre_gain, docs, query_weight, key_weight, value_weight)
+    )(stream, of(pre_gain, 0), docs, of(query_weight, 0), of(key_weight, 0), of(value_weight, 0))
     low, high = neighbours(kv)
     doc_rows = (low[tokens:], kv[tokens:], high[tokens:])
 
@@ -231,7 +245,7 @@
 
     attended = lax.all_gather(attention(0, query, kv, low, high), "tp", axis=0)
     branch = call(first_out, struct((tokens + pad, feat), bf16), [VMEM] * 3, "first_out")(
-        attended, out_weight, post_gain
+        attended, of(out_weight, 0), of(post_gain, 0)
     )
     branch = lax.all_gather(branch, "tp", axis=0)
     query, kv, own = call(
@@ -243,7 +257,16 @@
         ),
         [SMEM] + [VMEM] * 7,
         "next_heads",
-    )(at, stream, branch, pre_gain, post_gain, query_weight, key_weight, value_weight)
+    )(
+        at,
+        stream,
+        branch,
+        of(pre_gain, 1),
+        of(post_gain, 0),
+        of(query_weight, 1),
+        of(key_weight, 1),
+        of(value_weight, 1),
+    )
     low, high = neighbours(kv)
     attended = lax.all_gather(attention(1, query, kv, low, high), "tp", axis=0)
     branch, squares = call(
@@ -251,11 +274,11 @@
         (struct((tokens, feat), f32), struct((members, 1, tokens), f32)),
         [VMEM] * 2,
         "last_out",
-    )(attended, out_weight)
+    )(attended, of(out_weight, 1))
     squares = lax.all_to_all(squares, "tp", 0, 0, tiled=True)
     return call(
-        functools.partial(finish, model_width), struct((tokens, feat), bf16), [VMEM] * 4, "finish"
-    )(squares, branch, own, post_gain)
+        functools.partial(finish, model_width), jax.ShapeDtypeStruct((tokens, feat), bf16), [VMEM] * 4, "finish"
+    )(squares, branch, own, of(post_gain, 1))
 
 
 def solution(mesh):

time: 136 us -> 119 us (0.88)
  the two profiles are of different devices: /device:TPU:513 before, /device:TPU:199 now
where the time goes in v2:
time: 119 us
  blocking collectives  83.6 us (70%)
  starting transfers between devices  12.3 us (10%)
  waiting for transfers between devices  10.3 us (9%)
  Pallas kernels  6.7 us (6%)
  local copies, waits for them, and re-layouts  4.83 us (4%)
    all_gather x1, blocking collectives, shards(): stream = lax.all_gather(grid_in, 'tp', axis=0)  19.6 us
    all_gather x1, blocking collectives, shards(): attended = lax.all_gather(attention(0, query, kv, low, high), 'tp', axis=0)  17.8 us
    all_gather x1, blocking collectives, shards(): attended = lax.all_gather(attention(1, query, kv, low, high), 'tp', axis=0)  17.2 us
    all_gather x1, blocking collectives, shards(): branch = lax.all_gather(branch, 'tp', axis=0)  17.1 us
    all_to_all x1, blocking collectives, shards(): squares = lax.all_to_all(squares, 'tp', 0, 0, tiled=True)  11.9 us
    ppermute x2, waiting for transfers between devices, neighbours(): lax.ppermute(block, 'sp', backward)  10.3 us
    ppermute x2, starting transfers between devices, neighbours(): lax.ppermute(block, 'sp', forward)  7.04 us
    pallas_call x7, Pallas kernels, run(): kernel(*(pltpu.with_memory_space_constraint(arg, pltpu.VMEM) if spec is V...  6.7 us
  transfers between devices with their start and end apart: 4, of which 3 were waited for; matrix products, arithmetic and copies ran while one was open for 1% of the time, Pallas kernels for 0%

profile of v2, /device:TPU:199, one launch (start us, length us, event | category | flops | bytes accessed | tf_op | source)
XLA Modules:
  0.0 118.6 jit_solution(5949568156310960814)
XLA Ops:
  0.0 2.2 %fusion.3 = (bf16[1,2048,128]{2,1,0:T(8,128)(2,1)}, bf16[1,2048,128]{2,1,0:T(8,128)(2,1)S(1)}) fusion(bf16[2,2048,128]{2,1,0:T(8,128)(2,1)} %param.12), kind=kLoop, calls=%fused_computation.4 | loop fusion | bytes 2097152 | tf_op jit(solution)/shard_map/slice | solution.py:49
  2.2 0.0 copy-done.7
  2.2 19.6 %all-gather = bf16[2048,128]{1,0:T(8,128)(2,1)S(1)} all-gather(bf16[128,128]{1,0:T(8,128)(2,1)S(1)} %copy-done.7), channel_id=2, replica_groups=mesh['sp'=48,'tp'=16] {'tp'}, dimensions={0}, use_global_device_ids=true | all-gather | bytes 557056 | tf_op jit(solution)/shard_map/all_gather | solution.py:228
  21.9 1.1 fusion.1
  23.1 0.7 copy-done.3
  23.7 0.6 first_heads.1
  24.3 5.1 %collective-permute-start = (bf16[144,256]{1,0:T(8,128)(2,1)S(1)}, bf16[144,256]{1,0:T(8,128)(2,1)S(1)}, u32[]{:S(2)}, u32[]{:S(2)}) collective-permute-start(bf16[144,256]{1,0:T(8,128)(2,1)S(1)} %get-tuple-element.13.own_ref), channel_id=1, source_target_pairs={{0,16},{16,32},{32,48},{48,64},{64,80},{80,96},{96,112},{112,128},... | collective-permute-start | bytes 221192 | tf_op jit(solution)/shard_map/ppermute | solution.py:200
  29.5 1.9 %collective-permute-start.1 = (bf16[144,256]{1,0:T(8,128)(2,1)S(1)}, bf16[144,256]{1,0:T(8,128)(2,1)S(1)}, u32[]{:S(2)}, u32[]{:S(2)}) collective-permute-start(bf16[144,256]{1,0:T(8,128)(2,1)S(1)} %get-tuple-element.13.own_ref), channel_id=1, source_target_pairs={{16,0},{32,16},{48,32},{64,48},{80,64},{96,80},{112,96},{128,112},... | collective-permute-start | bytes 221192 | tf_op jit(solution)/shard_map/ppermute | solution.py:200
  31.4 0.0 copy-done.8
  31.5 0.0 copy-start.10
  31.5 0.1 reshape.7.bias_ref
  31.6 0.6 copy-done.10
  32.1 0.1 fusion
  32.2 0.7 pad_add_fusion.at_ref
  32.9 0.0 collective-permute-done.low_ref
  32.9 5.0 %collective-permute-done.1.high_ref = bf16[144,256]{1,0:T(8,128)(2,1)S(1)} collective-permute-done((bf16[144,256]{1,0:T(8,128)(2,1)S(1)}, bf16[144,256]{1,0:T(8,128)(2,1)S(1)}, u32[]{:S(2)}, u32[]{:S(2)}) %collective-permute-start.1) | collective-permute-done | bytes 73760 | tf_op jit(solution)/shard_map/ppermute | solution.py:200
  37.9 1.6 %attend0.1 = bf16[128,128]{1,0:T(8,128)(2,1)S(1)} custom-call(s32[2]{0:T(128)} %pad_add_fusion.at_ref, bf16[128,128]{1,0:T(8,128)(2,1)S(1)} %get-tuple-element.12.q_ref, bf16[144,256]{1,0:T(8,128)(2,1)S(1)} %get-tuple-element.13.own_ref, bf16[144,256]{1,0:T(8,128)(2,1)S(1)} %collective-permute-done.low_ref, ...), custom_call_target="tpu_custom_call" | custom-call | tf_op jit(solution)/shard_map/attend0/pallas_call | solution.py:34
  39.5 17.8 %all-gather.1 = bf16[2048,128]{1,0:T(8,128)(2,1)S(1)} all-gather(bf16[128,128]{1,0:T(8,128)(2,1)S(1)} %attend0.1), channel_id=3, replica_groups=mesh['sp'=48,'tp'=16] {'tp'}, dimensions={0}, use_global_device_ids=true | all-gather | bytes 557056 | tf_op jit(solution)/shard_map/all_gather | solution.py:246
  57.3 0.3 first_out.1
  57.6 0.0 copy-start
  57.6 17.1 %all-gather.2 = bf16[2304,128]{1,0:T(8,128)(2,1)S(1)} all-gather(bf16[144,128]{1,0:T(8,128)(2,1)S(1)} %first_out.1), channel_id=4, replica_groups=mesh['sp'=48,'tp'=16] {'tp'}, dimensions={0}, use_global_device_ids=true | all-gather | bytes 626688 | tf_op jit(solution)/shard_map/all_gather | solution.py:250
  74.7 0.0 copy-done.2
  74.7 1.5 %next_heads.1 = (bf16[128,128]{1,0:T(8,128)(2,1)S(1)}, bf16[128,256]{1,0:T(8,128)(2,1)S(1)}, bf16[128,128]{1,0:T(8,128)(2,1)S(1)}) custom-call(s32[2]{0:T(128)} %pad_add_fusion.at_ref, bf16[16,128,128]{2,1,0:T(8,128)(2,1)S(1)} %bitcast.10, bf16[16,144,128]{2,1,0:T(8,128)(2,1)S(1)} %bitcast.11, f32[1,2048]{1,0:T(1,128)S(1)} %get-tuple-element.27.gain_ref, ...), custom_call_target="tpu_custom_call" | custom-call | tf_op jit(solution)/shard_map/next_heads/pallas_call | solution.py:34
  76.2 1.9 %collective-permute-start.2 = (bf16[128,256]{1,0:T(8,128)(2,1)S(1)}, bf16[128,256]{1,0:T(8,128)(2,1)S(1)}, u32[]{:S(2)}, u32[]{:S(2)}) collective-permute-start(bf16[128,256]{1,0:T(8,128)(2,1)S(1)} %get-tuple-element.15.own_ref), channel_id=1, source_target_pairs={{0,16},{16,32},{32,48},{48,64},{64,80},{80,96},{96,112},{112,128},... | collective-permute-start | bytes 196616 | tf_op jit(solution)/shard_map/ppermute | solution.py:200
  78.1 3.4 %collective-permute-start.3 = (bf16[128,256]{1,0:T(8,128)(2,1)S(1)}, bf16[128,256]{1,0:T(8,128)(2,1)S(1)}, u32[]{:S(2)}, u32[]{:S(2)}) collective-permute-start(bf16[128,256]{1,0:T(8,128)(2,1)S(1)} %get-tuple-element.15.own_ref), channel_id=1, source_target_pairs={{16,0},{32,16},{48,32},{64,48},{80,64},{96,80},{112,96},{128,112},... | collective-permute-start | bytes 196616 | tf_op jit(solution)/shard_map/ppermute | solution.py:200
  81.5 0.1 collective-permute-done.2.low_ref
  81.6 5.2 %collective-permute-done.3.high_ref = bf16[128,256]{1,0:T(8,128)(2,1)S(1)} collective-permute-done((bf16[128,256]{1,0:T(8,128)(2,1)S(1)}, bf16[128,256]{1,0:T(8,128)(2,1)S(1)}, u32[]{:S(2)}, u32[]{:S(2)}) %collective-permute-start.3) | collective-permute-done | bytes 65568 | tf_op jit(solution)/shard_map/ppermute | solution.py:200
  86.8 1.6 %attend1.1 = bf16[128,128]{1,0:T(8,128)(2,1)S(1)} custom-call(s32[2]{0:T(128)} %pad_add_fusion.at_ref, bf16[128,128]{1,0:T(8,128)(2,1)S(1)} %get-tuple-element.14.q_ref, bf16[128,256]{1,0:T(8,128)(2,1)S(1)} %get-tuple-element.15.own_ref, bf16[128,256]{1,0:T(8,128)(2,1)S(1)} %collective-permute-done.2.low_ref, ...), custom_call_target="tpu_custom_call" | custom-call | tf_op jit(solution)/shard_map/attend1/pallas_call | solution.py:34
  88.4 17.2 %all-gather.3 = bf16[2048,128]{1,0:T(8,128)(2,1)S(1)} all-gather(bf16[128,128]{1,0:T(8,128)(2,1)S(1)} %attend1.1), channel_id=5, replica_groups=mesh['sp'=48,'tp'=16] {'tp'}, dimensions={0}, use_global_device_ids=true | all-gather | bytes 557056 | tf_op jit(solution)/shard_map/all_gather | solution.py:271
  105.6 0.4 last_out.1
  106.0 11.9 %all_to_all.5.squares_ref = f32[16,1,128]{2,1,0:T(1,128)S(1)} all-to-all(f32[16,1,128]{2,1,0:T(1,128)S(1)} %get-tuple-element.16), channel_id=1, replica_groups=mesh['sp'=48,'tp'=16] {'tp'}, dimensions={0} | all-to-all | bytes 16384 | tf_op jit(solution)/shard_map/all_to_all | solution.py:278
  117.9 0.7 finish.1
  (22 shorter events, 0.1 us)
Async XLA Ops:
  0.0 2.2 %copy-start.7 = (bf16[128,128]{1,0:T(8,128)(2,1)S(1)}, bf16[128,128]{1,0:T(8,128)(2,1)}, u32[]{:S(2)}) copy-start(bf16[128,128]{1,0:T(8,128)(2,1)} %param.9) | copy-start | bytes 98308
  0.0 21.9 %copy-start.6 = (bf16[2,2048,128]{2,1,0:T(8,128)(2,1)S(1)}, bf16[2,2048,128]{2,1,0:T(8,128)(2,1)}, u32[]{:S(2)}) copy-start(bf16[2,2048,128]{2,1,0:T(8,128)(2,1)} %param.13) | copy-start | bytes 3145732
  0.0 21.9 %copy-start.5 = (bf16[2,2048,128]{2,1,0:T(8,128)(2,1)S(1)}, bf16[2,2048,128]{2,1,0:T(8,128)(2,1)}, u32[]{:S(2)}) copy-start(bf16[2,2048,128]{2,1,0:T(8,128)(2,1)} %param.14) | copy-start | bytes 3145732
  2.2 19.6 %copy-start.9 = (f32[2,2048]{1,0:T(2,128)S(1)}, f32[2,2048]{1,0:T(2,128)}, u32[]{:S(2)}) copy-start(f32[2,2048]{1,0:T(2,128)} %param.11) | copy-start | bytes 49156
  23.1 0.7 copy-start.3
  23.7 7.7 %copy-start.8 = (f32[2,2,15,31]{3,1,2,0:T(2,128)S(1)}, f32[2,2,15,31]{3,1,2,0:T(2,128)}, u32[]{:S(2)}) copy-start(f32[2,2,15,31]{3,1,2,0:T(2,128)} %param.15) | copy-start | bytes 22324
  23.7 8.4 %copy-start.4 = (bf16[2,2048,128]{2,1,0:T(8,128)(2,1)S(1)}, bf16[2,2048,128]{2,1,0:T(8,128)(2,1)}, u32[]{:S(2)}) copy-start(bf16[2,2048,128]{2,1,0:T(8,128)(2,1)} %param.16) | copy-start | bytes 3145732
  24.3 8.5 %collective-permute-start = (bf16[144,256]{1,0:T(8,128)(2,1)S(1)}, bf16[144,256]{1,0:T(8,128)(2,1)S(1)}, u32[]{:S(2)}, u32[]{:S(2)}) collective-permute-start(bf16[144,256]{1,0:T(8,128)(2,1)S(1)} %get-tuple-element.13.own_ref), channel_id=1, source_target_pairs={{0,16},{16,32},{32,48},{48,64},{64,80},{80,96},{96,112},{112,128},... | collective-permute-start | bytes 221192 | tf_op jit(solution)/shard_map/ppermute | solution.py:200
  29.5 8.4 %collective-permute-start.1 = (bf16[144,256]{1,0:T(8,128)(2,1)S(1)}, bf16[144,256]{1,0:T(8,128)(2,1)S(1)}, u32[]{:S(2)}, u32[]{:S(2)}) collective-permute-start(bf16[144,256]{1,0:T(8,128)(2,1)S(1)} %get-tuple-element.13.own_ref), channel_id=1, source_target_pairs={{16,0},{32,16},{48,32},{64,48},{80,64},{96,80},{112,96},{128,112},... | collective-permute-start | bytes 221192 | tf_op jit(solution)/shard_map/ppermute | solution.py:200
  31.5 0.7 copy-start.10
  57.3 17.4 %copy-start.1 = (bf16[1,2048,128]{2,1,0:T(8,128)(2,1)S(1)}, bf16[1,2048,128]{2,1,0:T(8,128)(2,1)}, u32[]{:S(2)}) copy-start(bf16[1,2048,128]{2,1,0:T(8,128)(2,1)} %get-tuple-element.21.wv_ref) | copy-start | bytes 1572868
  57.3 17.4 %copy-start.2 = (bf16[1,2048,128]{2,1,0:T(8,128)(2,1)S(1)}, bf16[1,2048,128]{2,1,0:T(8,128)(2,1)}, u32[]{:S(2)}) copy-start(bf16[1,2048,128]{2,1,0:T(8,128)(2,1)} %get-tuple-element.32.wk_ref) | copy-start | bytes 1572868
  57.6 17.1 %copy-start = (bf16[1,2048,128]{2,1,0:T(8,128)(2,1)S(1)}, bf16[1,2048,128]{2,1,0:T(8,128)(2,1)}, u32[]{:S(2)}) copy-start(bf16[1,2048,128]{2,1,0:T(8,128)(2,1)} %get-tuple-element.25.wq_ref) | copy-start | bytes 1572868
  76.2 5.4 %collective-permute-start.2 = (bf16[128,256]{1,0:T(8,128)(2,1)S(1)}, bf16[128,256]{1,0:T(8,128)(2,1)S(1)}, u32[]{:S(2)}, u32[]{:S(2)}) collective-permute-start(bf16[128,256]{1,0:T(8,128)(2,1)S(1)} %get-tuple-element.15.own_ref), channel_id=1, source_target_pairs={{0,16},{16,32},{32,48},{48,64},{64,80},{80,96},{96,112},{112,128},... | collective-permute-start | bytes 196616 | tf_op jit(solution)/shard_map/ppermute | solution.py:200
  78.1 8.7 %collective-permute-start.3 = (bf16[128,256]{1,0:T(8,128)(2,1)S(1)}, bf16[128,256]{1,0:T(8,128)(2,1)S(1)}, u32[]{:S(2)}, u32[]{:S(2)}) collective-permute-start(bf16[128,256]{1,0:T(8,128)(2,1)S(1)} %get-tuple-element.15.own_ref), channel_id=1, source_target_pairs={{16,0},{32,16},{48,32},{64,48},{80,64},{96,80},{112,96},{128,112},... | collective-permute-start | bytes 196616 | tf_op jit(solution)/shard_map/ppermute | solution.py:200

commit v3 on v1

v3 whole, which is shorter than its diff:
```python
import functools

import jax
import jax.numpy as jnp
from jax import lax
from jax.experimental import pallas as pl
from jax.experimental.pallas import tpu as pltpu
from jax.sharding import PartitionSpec as P

HEAD_DIM = 64
WIN_ROWS = 8
WIN_COLS = 16
GRID_W = 32
LAYERS = 2
EPSILON = 1e-06
RIM = WIN_ROWS // 2
BIAS_ROWS = 2 * WIN_ROWS
LOWEST = -1e30
PAD = 16

VMEM = pl.BlockSpec(memory_space=pltpu.VMEM)
SMEM = pl.BlockSpec(memory_space=pltpu.SMEM)
HBM = pl.BlockSpec(memory_space=pltpu.HBM)


def call(body, outs, specs, name, scratch=()):
    kernel = pl.pallas_call(
        body,
        out_shape=outs,
        in_specs=specs,
        out_specs=jax.tree.map(lambda _: VMEM, outs),
        scratch_shapes=scratch,
        compiler_params=pltpu.CompilerParams(vmem_limit_bytes=16 << 20),
        name=name,
    )

    def run(*args):
        return kernel(
            *(
                arg if spec is SMEM else pltpu.with_memory_space_constraint(arg, spec.memory_space)
                for arg, spec in zip(args, specs, strict=True)
            )
        )

    return run


def copying(pairs, sems):
    copies = [pltpu.make_async_copy(src, dst, sems.at[i]) for i, (src, dst) in enumerate(pairs)]
    for copy in copies:
        copy.start()
    return copies


def as_column(row, size):
    return jnp.transpose(jnp.broadcast_to(row, (size, size)))


def lanes(i, width):
    return slice(i * width, (i + 1) * width)


def key_value(scaled, scaler, wk, wv, kv_ref):
    tokens, cols = scaled.shape[0], wk.shape[1]
    both = jnp.dot(scaled, jnp.concatenate([wk, wv], axis=1), preferred_element_type=jnp.float32)
    scaler = jnp.concatenate([scaler] * (2 * cols // scaler.shape[1]), axis=1)
    kv_ref[:tokens] = (both * scaler).astype(jnp.bfloat16)


def scaler_of(squares, model_width):
    total = jnp.sum(squares, axis=1, keepdims=True)
    return jnp.broadcast_to(lax.rsqrt(total / model_width + EPSILON), squares.shape)


def first_heads(
    x_ref, gain_hbm, docs_hbm, wk_hbm, wv_hbm,
    kv_ref, scaled_ref, scaler_ref, gain_ref, docs_ref, wk_ref, wv_ref, sems,
):
    copies = copying(
        (
            (gain_hbm, gain_ref),
            (docs_hbm, docs_ref),
            (wk_hbm.at[0], wk_ref),
            (wv_hbm.at[0], wv_ref),
        ),
        sems,
    )
    count, tokens, feat = x_ref.shape
    squares = jnp.zeros((tokens, feat), jnp.float32)
    copies[0].wait()
    for i in range(count):
        wide = x_ref[i].astype(jnp.float32)
        squares += wide * wide
        scaled_ref[:, lanes(i, feat)] = (wide * gain_ref[0:1, lanes(i, feat)]).astype(jnp.bfloat16)
    scaler = scaler_of(squares, count * feat)
    scaler_ref[...] = scaler
    copies[1].wait()
    row = docs_ref[...].astype(jnp.float32)
    row = jnp.concatenate([row] * (kv_ref.shape[1] // tokens), axis=1)
    kv_ref[tokens:] = jnp.broadcast_to(row, (kv_ref.shape[0] - tokens, kv_ref.shape[1])).astype(jnp.bfloat16)
    copies[2].wait()
    copies[3].wait()
    key_value(scaled_ref[...], scaler, wk_ref[...], wv_ref[...], kv_ref)


def query_from(scaled_ref, scaler_ref, wq):
    query = jnp.dot(scaled_ref[...], wq, preferred_element_type=jnp.float32)
    return (query * scaler_ref[...]).astype(jnp.bfloat16)


def biases(last_row, first_row, flat_ref, bias_ref):
    heads, tokens, keys = bias_ref.shape
    rows = tokens // GRID_W
    width = flat_ref.shape[1]
    token = lax.broadcasted_iota(jnp.int32, (GRID_W, keys), 0)
    other = lax.broadcasted_iota(jnp.int32, (GRID_W, keys), 1)
    key_row, key_col = first_row - rows + other // GRID_W, other % GRID_W
    col_start = jnp.clip(token - WIN_COLS // 2, 0, GRID_W - WIN_COLS)
    near = (key_col >= col_start) & (key_col < col_start + WIN_COLS)
    for r in range(rows):
        row_start = jnp.clip(first_row + r - RIM, 0, last_row - WIN_ROWS)
        inside = near & (key_row >= row_start) & (key_row < row_start + WIN_ROWS)
        shift = (-(WIN_COLS - 1) - (WIN_ROWS - 1 - rows - r) * GRID_W) % width
        for head in range(heads):
            flat = jnp.broadcast_to(flat_ref[head : head + 1], (GRID_W, width))
            turned = pltpu.roll(flat, shift, 1, stride=1, stride_axis=0)[:, :keys]
            bias_ref[head, lanes(r, GRID_W)] = jnp.where(inside, turned, LOWEST)


def first_query(
    last_row, at_ref, scaled_ref, scaler_ref, flat_ref, wq_hbm, wk_hbm, wv_hbm, wo_hbm, post_hbm,
    q_ref, bias_ref, wk_ref, wv_ref, wo_ref, post_ref, wq_ref, sems,
):
    copies = copying(
        (
            (wq_hbm.at[0], wq_ref),
            (wo_hbm.at[0], wo_ref),
            (post_hbm, post_ref),
            (wk_hbm.at[1], wk_ref),
            (wv_hbm.at[1], wv_ref),
        ),
        sems,
    )
    biases(last_row, at_ref[1] * (scaled_ref.shape[0] // GRID_W), flat_ref.at[0], bias_ref)
    copies[0].wait()
    q_ref[...] = query_from(scaled_ref, scaler_ref, wq_ref[...])
    for copy in copies[1:]:
        copy.wait()


def next_query(
    last_row, at_ref, scaled_ref, scaler_ref, flat_ref, wq_hbm, wo_hbm,
    q_ref, bias_ref, wo_ref, wq_ref, sems,
):
    copies = copying(((wq_hbm.at[1], wq_ref), (wo_hbm.at[1], wo_ref)), sems)
    biases(last_row, at_ref[1] * (scaled_ref.shape[0] // GRID_W), flat_ref.at[1], bias_ref)
    copies[0].wait()
    q_ref[...] = query_from(scaled_ref, scaler_ref, wq_ref[...])
    copies[1].wait()


def next_heads(
    at_ref, x_ref, b_ref, gain_ref, post_ref, wk_ref, wv_ref, kv_ref, scaled_ref, scaler_ref, own_ref
):
    count, tokens, feat = x_ref.shape
    squares = jnp.zeros((tokens, feat), jnp.float32)
    for i in range(count):
        branch = b_ref[i, :tokens].astype(jnp.float32)
        squares += branch * branch
    scale = scaler_of(squares, count * feat)
    squares = jnp.zeros((tokens, feat), jnp.float32)
    for i in range(count):
        parts = b_ref[i, tokens:].astype(jnp.float32)
        post = parts[0:1] + parts[1:2] + parts[2:3]
        branch = b_ref[i, :tokens].astype(jnp.float32)
        stream = (x_ref[i].astype(jnp.float32) + branch * scale * post).astype(jnp.bfloat16)
        wide = stream.astype(jnp.float32)
        squares += wide * wide
        scaled_ref[:, lanes(i, feat)] = (wide * gain_ref[1:2, lanes(i, feat)]).astype(jnp.bfloat16)
    scaler = scaler_of(squares, count * feat)
    scaler_ref[...] = scaler
    at = at_ref[0]
    own = x_ref[at].astype(jnp.float32)
    own_branch = b_ref[at][:tokens].astype(jnp.float32)
    own_ref[...] = (own + own_branch * scale * post_ref[0:1]).astype(jnp.bfloat16)
    key_value(scaled_ref[...], scaler, wk_ref[...], wv_ref[...], kv_ref)


def attend(q_ref, own_ref, low_ref, high_ref, dl_ref, do_ref, dh_ref, bias_ref, out_ref):
    tokens, cols = q_ref.shape
    heads = cols // HEAD_DIM
    blocks = (low_ref, own_ref, high_ref)
    key = jnp.concatenate([b[:tokens, :cols] for b in blocks], axis=0)
    value = jnp.concatenate([b[:tokens, cols:] for b in blocks], axis=0)
    key_docs = jnp.concatenate(
        [d[:1, :tokens].astype(jnp.float32) for d in (dl_ref, do_ref, dh_ref)], axis=1
    )
    query_docs = as_column(do_ref[:1, :tokens].astype(jnp.float32), tokens)
    same = key_docs == jnp.concatenate([query_docs] * 3, axis=1)
    query = q_ref[...]
    lane = lax.broadcasted_iota(jnp.int32, (tokens, cols), 1)
    split = jnp.concatenate(
        [jnp.where(lane // HEAD_DIM == h, query, jnp.zeros_like(query)) for h in range(heads)], axis=0
    )
    products = lax.dot_general(
        split, key, (((1,), (1,)), ((), ())), preferred_element_type=jnp.float32
    )
    lifted = []
    for h in range(heads):
        scores = products[lanes(h, tokens)] * HEAD_DIM ** (-0.5) + bias_ref[h]
        scores = jnp.where(same, scores, LOWEST)
        lifted.append(jnp.exp(scores - jnp.max(scores, axis=1, keepdims=True)))
    lifted = jnp.concatenate(lifted, axis=0)
    summed = jnp.dot(lifted.astype(jnp.bfloat16), value, preferred_element_type=jnp.float32)
    summed = summed / jnp.sum(lifted, axis=1, keepdims=True)
    result = summed[:tokens]
    for h in range(1, heads):
        result = jnp.where(lane // HEAD_DIM == h, summed[lanes(h, tokens)], result)
    out_ref[...] = result.astype(jnp.bfloat16)


def projected(a_ref, w_ref):
    joined = jnp.concatenate([a_ref[i] for i in range(a_ref.shape[0])], axis=1)
    return jnp.dot(joined, w_ref[...], preferred_element_type=jnp.float32)


def first_out(a_ref, w_ref, post_ref, out_ref):
    tokens = a_ref.shape[1]
    out_ref[:tokens] = projected(a_ref, w_ref).astype(jnp.bfloat16)
    post = post_ref[0:1]
    high = post.astype(jnp.bfloat16).astype(jnp.float32)
    middle = (post - high).astype(jnp.bfloat16).astype(jnp.float32)
    low = post - high - middle
    place = lax.broadcasted_iota(jnp.int32, (out_ref.shape[0] - tokens, post.shape[1]), 0)
    rows = jnp.where(place == 0, high, jnp.where(place == 1, middle, low))
    out_ref[tokens:] = rows.astype(jnp.bfloat16)


def last_out(a_ref, w_ref, branch_ref, squares_ref):
    branch = projected(a_ref, w_ref)
    branch_ref[...] = branch
    squares = jnp.sum(jnp.transpose(branch * branch), axis=0, keepdims=True)
    squares_ref[...] = jnp.broadcast_to(squares[None], squares_ref.shape)


def finish(model_width, squares_ref, branch_ref, own_ref, post_ref, out_ref):
    total = jnp.sum(squares_ref[...], axis=0)
    scale = as_column(lax.rsqrt(total / model_width + EPSILON), branch_ref.shape[0])
    out_ref[...] = (
        own_ref[...].astype(jnp.float32) + branch_ref[...] * scale * post_ref[1:2]
    ).astype(jnp.bfloat16)


def neighbours(block):
    count = lax.axis_size("sp")
    forward = [(i, i + 1) for i in range(count - 1)]
    backward = [(i + 1, i) for i in range(count - 1)]
    return lax.ppermute(block, "sp", forward), lax.ppermute(block, "sp", backward)


def gathered(block):
    return lax.all_gather(block, "tp", axis=0)


def shards(
    grid_in,
    documents,
    pre_gain,
    query_weight,
    key_weight,
    value_weight,
    offset_bias,
    out_weight,
    post_gain,
):
    tokens, feat = grid_in.shape
    _, model_width, cols = query_weight.shape
    heads = offset_bias.shape[1]
    bf16, f32 = jnp.bfloat16, jnp.float32
    members = lax.axis_size("tp")
    all_rows = tokens // GRID_W * lax.axis_size("sp")
    at = jnp.stack([lax.axis_index("tp"), lax.axis_index("sp")]).astype(jnp.int32)
    flat = jnp.pad(
        offset_bias, ((0, 0), (0, 0), (0, BIAS_ROWS - 2 * WIN_ROWS + 1), (0, GRID_W - 2 * WIN_COLS + 1))
    ).reshape(LAYERS, heads, BIAS_ROWS * GRID_W)
    weight = pltpu.VMEM((model_width, cols), bf16)
    shared = (pltpu.VMEM((tokens, model_width), bf16), pltpu.VMEM((tokens, feat), f32))

    stream = gathered(grid_in)
    kv, scaled, scaler, gain = call(
        first_heads,
        (pltpu.VMEM((tokens + PAD, 2 * cols), bf16), *shared, pltpu.VMEM(pre_gain.shape, f32)),
        [VMEM] + [HBM] * 4,
        "first_heads",
        [pltpu.VMEM((1, tokens), jnp.int32), weight, weight, pltpu.SemaphoreType.DMA((4,))],
    )(stream, pre_gain, documents.reshape(1, tokens), key_weight, value_weight)
    low, high = neighbours(kv)
    bias_of = pltpu.VMEM((heads, tokens, 3 * tokens), f32)
    query, bias, wk, wv, out, post = call(
        functools.partial(first_query, all_rows),
        (
            pltpu.VMEM((tokens, cols), bf16),
            bias_of,
            *[weight] * 3,
            pltpu.VMEM(post_gain.shape, f32),
        ),
        [SMEM, VMEM, VMEM, VMEM] + [HBM] * 5,
        "first_query",
        [weight, pltpu.SemaphoreType.DMA((5,))],
    )(at, scaled, scaler, flat, query_weight, key_weight, value_weight, out_weight, post_gain)
    doc_rows = (low[tokens:], kv[tokens:], high[tokens:])

    def attention(query, kv, low, high, bias):
        return call(attend, pltpu.VMEM((tokens, cols), bf16), [VMEM] * 8, "attend")(
            query, kv, low, high, *doc_rows, bias
        )

    attended = gathered(attention(query, kv, low, high, bias))
    branch = call(first_out, pltpu.VMEM((tokens + PAD, feat), bf16), [VMEM] * 3, "first_out")(
        attended, out, post
    )
    branch = gathered(branch)
    kv, scaled, scaler, own = call(
        next_heads,
        (pltpu.VMEM((tokens, 2 * cols), bf16), *shared, pltpu.VMEM((tokens, feat), bf16)),
        [SMEM] + [VMEM] * 6,
        "next_heads",
    )(at, stream, branch, gain, post, wk, wv)
    low, high = neighbours(kv)
    query, bias, out = call(
        functools.partial(next_query, all_rows),
        (pltpu.VMEM((tokens, cols), bf16), bias_of, weight),
        [SMEM] + [VMEM] * 3 + [HBM] * 2,
        "next_query",
        [weight, pltpu.SemaphoreType.DMA((2,))],
    )(at, scaled, scaler, flat, query_weight, out_weight)
    attended = gathered(attention(query, kv, low, high, bias))
    branch, squares = call(
        last_out,
        (pltpu.VMEM((tokens, feat), f32), pltpu.VMEM((members, 1, tokens), f32)),
        [VMEM] * 2,
        "last_out",
    )(attended, out)
    squares = lax.all_to_all(squares, "tp", 0, 0, tiled=True)
    return call(
        functools.partial(finish, model_width),
        jax.ShapeDtypeStruct((tokens, feat), bf16),
        [VMEM] * 4,
        "finish",
    )(squares, branch, own, post)


def solution(mesh):
    return jax.shard_map(
        shards,
        mesh=mesh,
        in_specs=(
            P("sp", "tp"),
            P("sp"),
            P(),
            P(None, None, "tp"),
            P(None, None, "tp"),
            P(None, None, "tp"),
            P(None, "tp", None, None),
            P(None, None, "tp"),
            P(None, "tp"),
        ),
        out_specs=P("sp", "tp"),
        check_vma=False,
    )
```

time: 136 us -> 113 us (0.83)
  the two profiles are of different devices: /device:TPU:513 before, /device:TPU:199 now
where the time goes in v3:
time: 113 us
  blocking collectives  84 us (74%)
  starting transfers between devices  12.3 us (11%)
  Pallas kernels  9.43 us (8%)
  waiting for transfers between devices  6.95 us (6%)
    all_gather x4, blocking collectives, gathered(): return lax.all_gather(block, 'tp', axis=0)  72.2 us
    all_to_all x1, blocking collectives, shards(): squares = lax.all_to_all(squares, 'tp', 0, 0, tiled=True)  11.9 us
    pallas_call x9, Pallas kernels, run(): kernel(*(arg if spec is SMEM else pltpu.with_memory_space_constraint(arg,...  9.43 us
    ppermute x2, starting transfers between devices, neighbours(): lax.ppermute(block, 'sp', forward)  7.05 us
    ppermute x2, waiting for transfers between devices, neighbours(): lax.ppermute(block, 'sp', backward)  6.94 us
    ppermute x2, starting transfers between devices, neighbours(): lax.ppermute(block, 'sp', backward)  5.28 us
  transfers between devices with their start and end apart: 4, of which 2 were waited for; matrix products, arithmetic and copies ran while one was open for 0% of the time, Pallas kernels for 4%

profile of v3, /device:TPU:199, one launch (start us, length us, event | category | flops | bytes accessed | tf_op | source)
XLA Modules:
  0.0 113.1 jit_solution(11620864634527077726)
XLA Ops:
  0.0 19.8 %all-gather = bf16[2048,128]{1,0:T(8,128)(2,1)S(1)} all-gather(bf16[128,128]{1,0:T(8,128)(2,1)} %param.9), channel_id=2, replica_groups=mesh['sp'=48,'tp'=16] {'tp'}, dimensions={0}, use_global_device_ids=true | all-gather | bytes 557056 | tf_op jit(solution)/shard_map/all_gather | solution.py:262
  19.8 0.0 copy-start
  19.8 1.6 %first_heads.1 = (bf16[144,256]{1,0:T(8,128)(2,1)S(1)}, bf16[128,2048]{1,0:T(8,128)(2,1)S(1)}, f32[128,128]{1,0:T(8,128)S(1)}, f32[2,2048]{1,0:T(2,128)S(1)}) custom-call(bf16[16,128,128]{2,1,0:T(8,128)(2,1)S(1)} %bitcast.9, f32[2,2048]{1,0:T(2,128)} %gain_hbm.1, s32[1,128]{1,0:T(1,128)} %bitcast.14, bf16[2,2048,128]{2,1,0:T(8,128)(2,1)} %wk_hbm.3, ...), custom_call_target="tpu_custom_call" | custom-call | tf_op jit(solution)/shard_map/first_heads/pallas_call | solution.py:38
  21.4 5.1 %collective-permute-start = (bf16[144,256]{1,0:T(8,128)(2,1)S(1)}, bf16[144,256]{1,0:T(8,128)(2,1)S(1)}, u32[]{:S(2)}, u32[]{:S(2)}) collective-permute-start(bf16[144,256]{1,0:T(8,128)(2,1)S(1)} %get-tuple-element.27.own_ref), channel_id=1, source_target_pairs={{0,16},{16,32},{32,48},{48,64},{64,80},{80,96},{96,112},{112,128},... | collective-permute-start | bytes 221192 | tf_op jit(solution)/shard_map/ppermute | solution.py:258
  26.5 1.9 %collective-permute-start.1 = (bf16[144,256]{1,0:T(8,128)(2,1)S(1)}, bf16[144,256]{1,0:T(8,128)(2,1)S(1)}, u32[]{:S(2)}, u32[]{:S(2)}) collective-permute-start(bf16[144,256]{1,0:T(8,128)(2,1)S(1)} %get-tuple-element.27.own_ref), channel_id=1, source_target_pairs={{16,0},{32,16},{48,32},{64,48},{80,64},{96,80},{112,96},{128,112},... | collective-permute-start | bytes 221192 | tf_op jit(solution)/shard_map/ppermute | solution.py:258
  28.4 0.0 copy-done
  28.5 0.1 reshape.7.flat_ref
  28.6 0.1 pad_add_fusion.at_ref
  28.6 2.2 %first_query.1 = (bf16[128,128]{1,0:T(8,128)(2,1)S(1)}, f32[2,128,384]{2,1,0:T(8,128)S(1)}, bf16[2048,128]{1,0:T(8,128)(2,1)S(1)}, bf16[2048,128]{1,0:T(8,128)(2...) custom-call(s32[2]{0:T(128)S(1)} %pad_add_fusion.at_ref, ...), custom_call_target="tpu_custom_call" | custom-call | tf_op jit(solution)/shard_map/first_query/pallas_call | solution.py:38
  30.9 0.0 collective-permute-done.low_ref
  30.9 4.0 %collective-permute-done.1.high_ref = bf16[144,256]{1,0:T(8,128)(2,1)S(1)} collective-permute-done((bf16[144,256]{1,0:T(8,128)(2,1)S(1)}, bf16[144,256]{1,0:T(8,128)(2,1)S(1)}, u32[]{:S(2)}, u32[]{:S(2)}) %collective-permute-start.1) | collective-permute-done | bytes 73760 | tf_op jit(solution)/shard_map/ppermute | solution.py:258
  34.9 0.5 attend.2
  35.4 17.8 %all-gather.1 = bf16[2048,128]{1,0:T(8,128)(2,1)S(1)} all-gather(bf16[128,128]{1,0:T(8,128)(2,1)S(1)} %attend.2), channel_id=3, replica_groups=mesh['sp'=48,'tp'=16] {'tp'}, dimensions={0}, use_global_device_ids=true | all-gather | bytes 557056 | tf_op jit(solution)/shard_map/all_gather | solution.py:262
  53.1 0.3 first_out.1
  53.4 17.0 %all-gather.2 = bf16[2304,128]{1,0:T(8,128)(2,1)S(1)} all-gather(bf16[144,128]{1,0:T(8,128)(2,1)S(1)} %first_out.1), channel_id=4, replica_groups=mesh['sp'=48,'tp'=16] {'tp'}, dimensions={0}, use_global_device_ids=true | all-gather | bytes 626688 | tf_op jit(solution)/shard_map/all_gather | solution.py:262
  70.4 1.3 %next_heads.1 = (bf16[128,256]{1,0:T(8,128)(2,1)S(1)}, bf16[128,2048]{1,0:T(8,128)(2,1)S(1)}, f32[128,128]{1,0:T(8,128)S(1)}, bf16[128,128]{1,0:T(8,128)(2,1)S(1)}) custom-call(s32[2]{0:T(128)S(1)} %pad_add_fusion.at_ref, bf16[16,128,128]{2,1,0:T(8,128)(2,1)S(1)} %bitcast.10, bf16[16,144,128]{2,1,0:T(8,128)(2,1)S(1)} %bitcast.11, ...), custom_call_target="tpu_custom_call" | custom-call | tf_op jit(solution)/shard_map/next_heads/pallas_call | solution.py:38
  71.7 1.9 %collective-permute-start.2 = (bf16[128,256]{1,0:T(8,128)(2,1)S(1)}, bf16[128,256]{1,0:T(8,128)(2,1)S(1)}, u32[]{:S(2)}, u32[]{:S(2)}) collective-permute-start(bf16[128,256]{1,0:T(8,128)(2,1)S(1)} %get-tuple-element.37.own_ref), channel_id=1, source_target_pairs={{0,16},{16,32},{32,48},{48,64},{64,80},{80,96},{96,112},{112,128},... | collective-permute-start | bytes 196616 | tf_op jit(solution)/shard_map/ppermute | solution.py:258
  73.6 3.4 %collective-permute-start.3 = (bf16[128,256]{1,0:T(8,128)(2,1)S(1)}, bf16[128,256]{1,0:T(8,128)(2,1)S(1)}, u32[]{:S(2)}, u32[]{:S(2)}) collective-permute-start(bf16[128,256]{1,0:T(8,128)(2,1)S(1)} %get-tuple-element.37.own_ref), channel_id=1, source_target_pairs={{16,0},{32,16},{48,32},{64,48},{80,64},{96,80},{112,96},{128,112},... | collective-permute-start | bytes 196616 | tf_op jit(solution)/shard_map/ppermute | solution.py:258
  77.0 2.0 %next_query.1 = (bf16[128,128]{1,0:T(8,128)(2,1)S(1)}, f32[2,128,384]{2,1,0:T(8,128)S(1)}, bf16[2048,128]{1,0:T(8,128)(2,1)S(1)}) custom-call(s32[2]{0:T(128)S(1)} %pad_add_fusion.at_ref, bf16[128,2048]{1,0:T(8,128)(2,1)S(1)} %get-tuple-element.34.scaled_ref, f32[128,128]{1,0:T(8,128)S(1)} %get-tuple-element.35.scaler_ref, ...), custom_call_target="tpu_custom_call" | custom-call | tf_op jit(solution)/shard_map/next_query/pallas_call | solution.py:38
  79.0 0.0 collective-permute-done.2.low_ref
  79.0 3.0 %collective-permute-done.3.high_ref = bf16[128,256]{1,0:T(8,128)(2,1)S(1)} collective-permute-done((bf16[128,256]{1,0:T(8,128)(2,1)S(1)}, bf16[128,256]{1,0:T(8,128)(2,1)S(1)}, u32[]{:S(2)}, u32[]{:S(2)}) %collective-permute-start.3) | collective-permute-done | bytes 65568 | tf_op jit(solution)/shard_map/ppermute | solution.py:258
  82.0 0.5 attend.3
  82.4 17.7 %all-gather.3 = bf16[2048,128]{1,0:T(8,128)(2,1)S(1)} all-gather(bf16[128,128]{1,0:T(8,128)(2,1)S(1)} %attend.3), channel_id=5, replica_groups=mesh['sp'=48,'tp'=16] {'tp'}, dimensions={0}, use_global_device_ids=true | all-gather | bytes 557056 | tf_op jit(solution)/shard_map/all_gather | solution.py:262
  100.1 0.4 last_out.1
  100.5 11.9 %all_to_all.5.squares_ref = f32[16,1,128]{2,1,0:T(1,128)S(1)} all-to-all(f32[16,1,128]{2,1,0:T(1,128)S(1)} %get-tuple-element.40), channel_id=1, replica_groups=mesh['sp'=48,'tp'=16] {'tp'}, dimensions={0} | all-to-all | bytes 16384 | tf_op jit(solution)/shard_map/all_to_all | solution.py:344
  112.4 0.7 finish.1
  (5 shorter events, 0.0 us)
Async XLA Ops:
  19.8 8.7 %copy-start = (f32[2,2,15,31]{3,1,2,0:T(2,128)S(1)}, f32[2,2,15,31]{3,1,2,0:T(2,128)}, u32[]{:S(2)}) copy-start(f32[2,2,15,31]{3,1,2,0:T(2,128)} %param.15) | copy-start | bytes 22324
  21.4 9.5 %collective-permute-start = (bf16[144,256]{1,0:T(8,128)(2,1)S(1)}, bf16[144,256]{1,0:T(8,128)(2,1)S(1)}, u32[]{:S(2)}, u32[]{:S(2)}) collective-permute-start(bf16[144,256]{1,0:T(8,128)(2,1)S(1)} %get-tuple-element.27.own_ref), channel_id=1, source_target_pairs={{0,16},{16,32},{32,48},{48,64},{64,80},{80,96},{96,112},{112,128},... | collective-permute-start | bytes 221192 | tf_op jit(solution)/shard_map/ppermute | solution.py:258
  26.5 8.4 %collective-permute-start.1 = (bf16[144,256]{1,0:T(8,128)(2,1)S(1)}, bf16[144,256]{1,0:T(8,128)(2,1)S(1)}, u32[]{:S(2)}, u32[]{:S(2)}) collective-permute-start(bf16[144,256]{1,0:T(8,128)(2,1)S(1)} %get-tuple-element.27.own_ref), channel_id=1, source_target_pairs={{16,0},{32,16},{48,32},{64,48},{80,64},{96,80},{112,96},{128,112},... | collective-permute-start | bytes 221192 | tf_op jit(solution)/shard_map/ppermute | solution.py:258
  71.7 7.3 %collective-permute-start.2 = (bf16[128,256]{1,0:T(8,128)(2,1)S(1)}, bf16[128,256]{1,0:T(8,128)(2,1)S(1)}, u32[]{:S(2)}, u32[]{:S(2)}) collective-permute-start(bf16[128,256]{1,0:T(8,128)(2,1)S(1)} %get-tuple-element.37.own_ref), channel_id=1, source_target_pairs={{0,16},{16,32},{32,48},{48,64},{64,80},{80,96},{96,112},{112,128},... | collective-permute-start | bytes 196616 | tf_op jit(solution)/shard_map/ppermute | solution.py:258
  73.6 8.3 %collective-permute-start.3 = (bf16[128,256]{1,0:T(8,128)(2,1)S(1)}, bf16[128,256]{1,0:T(8,128)(2,1)S(1)}, u32[]{:S(2)}, u32[]{:S(2)}) collective-permute-start(bf16[128,256]{1,0:T(8,128)(2,1)S(1)} %get-tuple-element.37.own_ref), channel_id=1, source_target_pairs={{16,0},{32,16},{48,32},{64,48},{80,64},{96,80},{112,96},{128,112},... | collective-permute-start | bytes 196616 | tf_op jit(solution)/shard_map/ppermute | solution.py:258

commit v4 on v3

--- a/solution.py
+++ b/solution.py
@@ -19,7 +19,6 @@
 PAD = 16
 
 VMEM = pl.BlockSpec(memory_space=pltpu.VMEM)
-SMEM = pl.BlockSpec(memory_space=pltpu.SMEM)
 HBM = pl.BlockSpec(memory_space=pltpu.HBM)
 
 
@@ -37,7 +36,7 @@
     def run(*args):
         return kernel(
             *(
-                arg if spec is SMEM else pltpu.with_memory_space_constraint(arg, spec.memory_space)
+                pltpu.with_memory_space_constraint(arg, spec.memory_space)
                 for arg, spec in zip(args, specs, strict=True)
             )
         )
@@ -108,27 +107,32 @@
     return (query * scaler_ref[...]).astype(jnp.bfloat16)
 
 
-def biases(last_row, first_row, flat_ref, bias_ref):
-    heads, tokens, keys = bias_ref.shape
+def biases(last_row, block, flat_ref, bias_ref):
+    blocks, heads, tokens, _ = bias_ref.shape
     rows = tokens // GRID_W
+    first_row = block * rows
     width = flat_ref.shape[1]
-    token = lax.broadcasted_iota(jnp.int32, (GRID_W, keys), 0)
-    other = lax.broadcasted_iota(jnp.int32, (GRID_W, keys), 1)
-    key_row, key_col = first_row - rows + other // GRID_W, other % GRID_W
+    token = lax.broadcasted_iota(jnp.int32, (GRID_W, tokens), 0)
+    other = lax.broadcasted_iota(jnp.int32, (GRID_W, tokens), 1)
+    row, col = other // GRID_W, other % GRID_W
     col_start = jnp.clip(token - WIN_COLS // 2, 0, GRID_W - WIN_COLS)
-    near = (key_col >= col_start) & (key_col < col_start + WIN_COLS)
-    for r in range(rows):
-        row_start = jnp.clip(first_row + r - RIM, 0, last_row - WIN_ROWS)
-        inside = near & (key_row >= row_start) & (key_row < row_start + WIN_ROWS)
-        shift = (-(WIN_COLS - 1) - (WIN_ROWS - 1 - rows - r) * GRID_W) % width
-        for head in range(heads):
-            flat = jnp.broadcast_to(flat_ref[head : head + 1], (GRID_W, width))
-            turned = pltpu.roll(flat, shift, 1, stride=1, stride_axis=0)[:, :keys]
-            bias_ref[head, lanes(r, GRID_W)] = jnp.where(inside, turned, LOWEST)
+    near = (col >= col_start) & (col < col_start + WIN_COLS)
+    for head in range(heads):
+        flat = jnp.broadcast_to(flat_ref[head : head + 1], (GRID_W, width))
+        turned = pltpu.roll(flat, width - (WIN_COLS - 1), 1, stride=1, stride_axis=0)
+        for r in range(rows):
+            start = jnp.clip(first_row + r - RIM, 0, last_row - WIN_ROWS) - first_row
+            skipped = (WIN_ROWS - 1 - rows - r) * GRID_W
+            for j in range(blocks):
+                key_row = row + (j - 1) * rows
+                inside = near & (key_row >= start) & (key_row < start + WIN_ROWS)
+                part = turned[:, skipped + j * tokens : skipped + (j + 1) * tokens]
+                place = jnp.where(block % 2 == 0, j, blocks - 1 - j)
+                bias_ref[place, head, lanes(r, GRID_W)] = jnp.where(inside, part, LOWEST)
 
 
 def first_query(
-    last_row, at_ref, scaled_ref, scaler_ref, flat_ref, wq_hbm, wk_hbm, wv_hbm, wo_hbm, post_hbm,
+    last_row, scaled_ref, scaler_ref, flat_ref, wq_hbm, wk_hbm, wv_hbm, wo_hbm, post_hbm,
     q_ref, bias_ref, wk_ref, wv_ref, wo_ref, post_ref, wq_ref, sems,
 ):
     copies = copying(
@@ -141,7 +145,7 @@
         ),
         sems,
     )
-    biases(last_row, at_ref[1] * (scaled_ref.shape[0] // GRID_W), flat_ref.at[0], bias_ref)
+    biases(last_row, lax.axis_index("sp"), flat_ref.at[0], bias_ref)
     copies[0].wait()
     q_ref[...] = query_from(scaled_ref, scaler_ref, wq_ref[...])
     for copy in copies[1:]:
@@ -149,18 +153,18 @@
 
 
 def next_query(
-    last_row, at_ref, scaled_ref, scaler_ref, flat_ref, wq_hbm, wo_hbm,
+    last_row, scaled_ref, scaler_ref, flat_ref, wq_hbm, wo_hbm,
     q_ref, bias_ref, wo_ref, wq_ref, sems,
 ):
     copies = copying(((wq_hbm.at[1], wq_ref), (wo_hbm.at[1], wo_ref)), sems)
-    biases(last_row, at_ref[1] * (scaled_ref.shape[0] // GRID_W), flat_ref.at[1], bias_ref)
+    biases(last_row, lax.axis_index("sp"), flat_ref.at[1], bias_ref)
     copies[0].wait()
     q_ref[...] = query_from(scaled_ref, scaler_ref, wq_ref[...])
     copies[1].wait()
 
 
 def next_heads(
-    at_ref, x_ref, b_ref, gain_ref, post_ref, wk_ref, wv_ref, kv_ref, scaled_ref, scaler_ref, own_ref
+    x_ref, b_ref, gain_ref, post_ref, wk_ref, wv_ref, kv_ref, scaled_ref, scaler_ref, own_ref
 ):
     count, tokens, feat = x_ref.shape
     squares = jnp.zeros((tokens, feat), jnp.float32)
@@ -179,21 +183,21 @@
         scaled_ref[:, lanes(i, feat)] = (wide * gain_ref[1:2, lanes(i, feat)]).astype(jnp.bfloat16)
     scaler = scaler_of(squares, count * feat)
     scaler_ref[...] = scaler
-    at = at_ref[0]
+    at = lax.axis_index("tp")
     own = x_ref[at].astype(jnp.float32)
     own_branch = b_ref[at][:tokens].astype(jnp.float32)
     own_ref[...] = (own + own_branch * scale * post_ref[0:1]).astype(jnp.bfloat16)
     key_value(scaled_ref[...], scaler, wk_ref[...], wv_ref[...], kv_ref)
 
 
-def attend(q_ref, own_ref, low_ref, high_ref, dl_ref, do_ref, dh_ref, bias_ref, out_ref):
+def attend(q_ref, own_ref, cross_ref, within_ref, dc_ref, do_ref, dw_ref, bias_ref, out_ref):
     tokens, cols = q_ref.shape
     heads = cols // HEAD_DIM
-    blocks = (low_ref, own_ref, high_ref)
+    blocks = (cross_ref, own_ref, within_ref)
     key = jnp.concatenate([b[:tokens, :cols] for b in blocks], axis=0)
     value = jnp.concatenate([b[:tokens, cols:] for b in blocks], axis=0)
     key_docs = jnp.concatenate(
-        [d[:1, :tokens].astype(jnp.float32) for d in (dl_ref, do_ref, dh_ref)], axis=1
+        [d[:1, :tokens].astype(jnp.float32) for d in (dc_ref, do_ref, dw_ref)], axis=1
     )
     query_docs = as_column(do_ref[:1, :tokens].astype(jnp.float32), tokens)
     same = key_docs == jnp.concatenate([query_docs] * 3, axis=1)
@@ -205,9 +209,10 @@
     products = lax.dot_general(
         split, key, (((1,), (1,)), ((), ())), preferred_element_type=jnp.float32
     )
+    bias = [jnp.concatenate([bias_ref[j, h] for j in range(len(blocks))], axis=1) for h in range(heads)]
     lifted = []
     for h in range(heads):
-        scores = products[lanes(h, tokens)] * HEAD_DIM ** (-0.5) + bias_ref[h]
+        scores = products[lanes(h, tokens)] * HEAD_DIM ** (-0.5) + bias[h]
         scores = jnp.where(same, scores, LOWEST)
         lifted.append(jnp.exp(scores - jnp.max(scores, axis=1, keepdims=True)))
     lifted = jnp.concatenate(lifted, axis=0)
@@ -253,9 +258,10 @@
 
 def neighbours(block):
     count = lax.axis_size("sp")
-    forward = [(i, i + 1) for i in range(count - 1)]
-    backward = [(i + 1, i) for i in range(count - 1)]
-    return lax.ppermute(block, "sp", forward), lax.ppermute(block, "sp", backward)
+    edges = [[(i, i + 1), (i + 1, i)] for i in range(count - 1)]
+    crossing = [pair for edge in edges[1::2] for pair in edge]
+    within = [pair for edge in edges[0::2] for pair in edge]
+    return lax.ppermute(block, "sp", crossing), lax.ppermute(block, "sp", within)
 
 
 def gathered(block):
@@ -279,7 +285,6 @@
     bf16, f32 = jnp.bfloat16, jnp.float32
     members = lax.axis_size("tp")
     all_rows = tokens // GRID_W * lax.axis_size("sp")
-    at = jnp.stack([lax.axis_index("tp"), lax.axis_index("sp")]).astype(jnp.int32)
     flat = jnp.pad(
         offset_bias, ((0, 0), (0, 0), (0, BIAS_ROWS - 2 * WIN_ROWS + 1), (0, GRID_W - 2 * WIN_COLS + 1))
     ).reshape(LAYERS, heads, BIAS_ROWS * GRID_W)
@@ -294,8 +299,8 @@
         "first_heads",
         [pltpu.VMEM((1, tokens), jnp.int32), weight, weight, pltpu.SemaphoreType.DMA((4,))],
     )(stream, pre_gain, documents.reshape(1, tokens), key_weight, value_weight)
-    low, high = neighbours(kv)
-    bias_of = pltpu.VMEM((heads, tokens, 3 * tokens), f32)
+    cross, within = neighbours(kv)
+    bias_of = pltpu.VMEM((3, heads, tokens, tokens), f32)
     query, bias, wk, wv, out, post = call(
         functools.partial(first_query, all_rows),
         (
@@ -304,18 +309,18 @@
             *[weight] * 3,
             pltpu.VMEM(post_gain.shape, f32),
         ),
-        [SMEM, VMEM, VMEM, VMEM] + [HBM] * 5,
+        [VMEM] * 3 + [HBM] * 5,
         "first_query",
         [weight, pltpu.SemaphoreType.DMA((5,))],
-    )(at, scaled, scaler, flat, query_weight, key_weight, value_weight, out_weight, post_gain)
-    doc_rows = (low[tokens:], kv[tokens:], high[tokens:])
-
-    def attention(query, kv, low, high, bias):
+    )(scaled, scaler, flat, query_weight, key_weight, value_weight, out_weight, post_gain)
+    doc_rows = (cross[tokens:], kv[tokens:], within[tokens:])
+
+    def attention(query, kv, cross, within, bias):
         return call(attend, pltpu.VMEM((tokens, cols), bf16), [VMEM] * 8, "attend")(
-            query, kv, low, high, *doc_rows, bias
+            query, kv, cross, within, *doc_rows, bias
         )
 
-    attended = gathered(attention(query, kv, low, high, bias))
+    attended = gathered(attention(query, kv, cross, within, bias))
     branch = call(first_out, pltpu.VMEM((tokens + PAD, feat), bf16), [VMEM] * 3, "first_out")(
         attended, out, post
     )
@@ -323,18 +328,18 @@
     kv, scaled, scaler, own = call(
         next_heads,
         (pltpu.VMEM((tokens, 2 * cols), bf16), *shared, pltpu.VMEM((tokens, feat), bf16)),
-        [SMEM] + [VMEM] * 6,
+        [VMEM] * 6,
         "next_heads",
-    )(at, stream, branch, gain, post, wk, wv)
-    low, high = neighbours(kv)
+    )(stream, branch, gain, post, wk, wv)
+    cross, within = neighbours(kv)
     query, bias, out = call(
         functools.partial(next_query, all_rows),
         (pltpu.VMEM((tokens, cols), bf16), bias_of, weight),
-        [SMEM] + [VMEM] * 3 + [HBM] * 2,
+        [VMEM] * 3 + [HBM] * 2,
         "next_query",
         [weight, pltpu.SemaphoreType.DMA((2,))],
-    )(at, scaled, scaler, flat, query_weight, out_weight)
-    attended = gathered(attention(query, kv, low, high, bias))
+    )(scaled, scaler, flat, query_weight, out_weight)
+    attended = gathered(attention(query, kv, cross, within, bias))
     branch, squares = call(
         last_out,
         (pltpu.VMEM((tokens, feat), f32), pltpu.VMEM((members, 1, tokens), f32)),

time: 113 us -> 108 us (0.956)
  the two profiles are of different devices: /device:TPU:199 before, /device:TPU:513 now
where the time goes in v4:
time: 108 us
  blocking collectives  83.6 us (77%)
  starting transfers between devices  12.6 us (12%)
  Pallas kernels  8.06 us (7%)
  waiting for transfers between devices  3.17 us (3%)
    all_gather x4, blocking collectives, gathered(): return lax.all_gather(block, 'tp', axis=0)  71.8 us
    all_to_all x1, blocking collectives, shards(): squares = lax.all_to_all(squares, 'tp', 0, 0, tiled=True)  11.9 us
    ppermute x2, starting transfers between devices, neighbours(): lax.ppermute(block, 'sp', crossing)  8.8 us
    pallas_call x9, Pallas kernels, run(): kernel(*(pltpu.with_memory_space_constraint(arg, spec.memory_space) for a...  8.06 us
    ppermute x2, starting transfers between devices, neighbours(): lax.ppermute(block, 'sp', within)  3.84 us
  transfers between devices with their start and end apart: 4, of which 2 were waited for; matrix products, arithmetic and copies ran while one was open for 0% of the time, Pallas kernels for 3%

profile of v4, /device:TPU:513, one launch (start us, length us, event | category | flops | bytes accessed | tf_op | source)
XLA Modules:
  0.0 107.8 jit_solution(16080649055498997348)
XLA Ops:
  0.0 19.8 %all-gather = bf16[2048,128]{1,0:T(8,128)(2,1)S(1)} all-gather(bf16[128,128]{1,0:T(8,128)(2,1)} %param.9), channel_id=2, replica_groups=mesh['sp'=48,'tp'=16] {'tp'}, dimensions={0}, use_global_device_ids=true | all-gather | bytes 557056 | tf_op jit(solution)/shard_map/all_gather | solution.py:268
  19.8 0.0 copy-start
  19.8 1.6 %first_heads.1 = (bf16[144,256]{1,0:T(8,128)(2,1)S(1)}, bf16[128,2048]{1,0:T(8,128)(2,1)S(1)}, f32[128,128]{1,0:T(8,128)S(1)}, f32[2,2048]{1,0:T(2,128)S(1)}) custom-call(bf16[16,128,128]{2,1,0:T(8,128)(2,1)S(1)} %bitcast.7, f32[2,2048]{1,0:T(2,128)} %gain_hbm.1, s32[1,128]{1,0:T(1,128)} %bitcast.12, bf16[2,2048,128]{2,1,0:T(8,128)(2,1)} %wk_hbm.3, ...), custom_call_target="tpu_custom_call" | custom-call | tf_op jit(solution)/shard_map/first_heads/pallas_call | solution.py:37
  21.4 5.6 %collective-permute-start = (bf16[144,256]{1,0:T(8,128)(2,1)S(1)}, bf16[144,256]{1,0:T(8,128)(2,1)S(1)}, u32[]{:S(2)}, u32[]{:S(2)}) collective-permute-start(bf16[144,256]{1,0:T(8,128)(2,1)S(1)} %get-tuple-element.27.own_ref), channel_id=1, source_target_pairs={{16,32},{32,16},{48,64},{64,48},{80,96},{96,80},{112,128},{128,112... | collective-permute-start | bytes 221192 | tf_op jit(solution)/shard_map/ppermute | solution.py:264
  27.0 1.9 %collective-permute-start.1 = (bf16[144,256]{1,0:T(8,128)(2,1)S(1)}, bf16[144,256]{1,0:T(8,128)(2,1)S(1)}, u32[]{:S(2)}, u32[]{:S(2)}) collective-permute-start(bf16[144,256]{1,0:T(8,128)(2,1)S(1)} %get-tuple-element.27.own_ref), channel_id=1, source_target_pairs={{0,16},{16,0},{32,48},{48,32},{64,80},{80,64},{96,112},{112,96},{1... | collective-permute-start | bytes 221192 | tf_op jit(solution)/shard_map/ppermute | solution.py:264
  28.9 0.0 copy-done
  28.9 0.1 reshape.7.flat_ref
  29.0 1.8 %first_query.1 = (bf16[128,128]{1,0:T(8,128)(2,1)S(1)}, f32[3,2,128,128]{3,2,1,0:T(8,128)S(1)}, bf16[2048,128]{1,0:T(8,128)(2,1)S(1)}, bf16[2048,128]{1,0:T(8,12...) custom-call(bf16[128,2048]{1,0:T(8,128)(2,1)S(1)} %get-tuple-element.24.scaled_ref, ...), custom_call_target="tpu_custom_call" | custom-call | tf_op jit(solution)/shard_map/first_query/pallas_call | solution.py:37
  30.8 0.0 collective-permute-done.cross_ref
  30.8 1.2 %collective-permute-done.1.within_ref = bf16[144,256]{1,0:T(8,128)(2,1)S(1)} collective-permute-done((bf16[144,256]{1,0:T(8,128)(2,1)S(1)}, bf16[144,256]{1,0:T(8,128)(2,1)S(1)}, u32[]{:S(2)}, u32[]{:S(2)}) %collective-permute-start.1) | collective-permute-done | bytes 73760 | tf_op jit(solution)/shard_map/ppermute | solution.py:264
  32.1 0.5 attend.2
  32.5 17.8 %all-gather.1 = bf16[2048,128]{1,0:T(8,128)(2,1)S(1)} all-gather(bf16[128,128]{1,0:T(8,128)(2,1)S(1)} %attend.2), channel_id=3, replica_groups=mesh['sp'=48,'tp'=16] {'tp'}, dimensions={0}, use_global_device_ids=true | all-gather | bytes 557056 | tf_op jit(solution)/shard_map/all_gather | solution.py:268
  50.3 0.3 first_out.1
  50.6 17.0 %all-gather.2 = bf16[2304,128]{1,0:T(8,128)(2,1)S(1)} all-gather(bf16[144,128]{1,0:T(8,128)(2,1)S(1)} %first_out.1), channel_id=4, replica_groups=mesh['sp'=48,'tp'=16] {'tp'}, dimensions={0}, use_global_device_ids=true | all-gather | bytes 626688 | tf_op jit(solution)/shard_map/all_gather | solution.py:268
  67.6 0.7 next_heads.1
  68.3 3.2 %collective-permute-start.2 = (bf16[128,256]{1,0:T(8,128)(2,1)S(1)}, bf16[128,256]{1,0:T(8,128)(2,1)S(1)}, u32[]{:S(2)}, u32[]{:S(2)}) collective-permute-start(bf16[128,256]{1,0:T(8,128)(2,1)S(1)} %get-tuple-element.37.own_ref), channel_id=1, source_target_pairs={{16,32},{32,16},{48,64},{64,48},{80,96},{96,80},{112,128},{128,112... | collective-permute-start | bytes 196616 | tf_op jit(solution)/shard_map/ppermute | solution.py:264
  71.5 1.9 %collective-permute-start.3 = (bf16[128,256]{1,0:T(8,128)(2,1)S(1)}, bf16[128,256]{1,0:T(8,128)(2,1)S(1)}, u32[]{:S(2)}, u32[]{:S(2)}) collective-permute-start(bf16[128,256]{1,0:T(8,128)(2,1)S(1)} %get-tuple-element.37.own_ref), channel_id=1, source_target_pairs={{0,16},{16,0},{32,48},{48,32},{64,80},{80,64},{96,112},{112,96},{1... | collective-permute-start | bytes 196616 | tf_op jit(solution)/shard_map/ppermute | solution.py:264
  73.5 1.6 %next_query.1 = (bf16[128,128]{1,0:T(8,128)(2,1)S(1)}, f32[3,2,128,128]{3,2,1,0:T(8,128)S(1)}, bf16[2048,128]{1,0:T(8,128)(2,1)S(1)}) custom-call(bf16[128,2048]{1,0:T(8,128)(2,1)S(1)} %get-tuple-element.34.scaled_ref, f32[128,128]{1,0:T(8,128)S(1)} %get-tuple-element.35.scaler_ref, f32[2,2,512]{2,1,0:T(2,128)S(1)} %reshape.7.flat_ref, ...), custom_call_target="tpu_custom_call" | custom-call | tf_op jit(solution)/shard_map/next_query/pallas_call | solution.py:37
  75.1 2.0 %collective-permute-done.2.cross_ref = bf16[128,256]{1,0:T(8,128)(2,1)S(1)} collective-permute-done((bf16[128,256]{1,0:T(8,128)(2,1)S(1)}, bf16[128,256]{1,0:T(8,128)(2,1)S(1)}, u32[]{:S(2)}, u32[]{:S(2)}) %collective-permute-start.2) | collective-permute-done | bytes 65568 | tf_op jit(solution)/shard_map/ppermute | solution.py:264
  77.0 0.0 collective-permute-done.3.within_ref
  77.0 0.5 attend.3
  77.5 17.3 %all-gather.3 = bf16[2048,128]{1,0:T(8,128)(2,1)S(1)} all-gather(bf16[128,128]{1,0:T(8,128)(2,1)S(1)} %attend.3), channel_id=5, replica_groups=mesh['sp'=48,'tp'=16] {'tp'}, dimensions={0}, use_global_device_ids=true | all-gather | bytes 557056 | tf_op jit(solution)/shard_map/all_gather | solution.py:268
  94.8 0.4 last_out.1
  95.1 11.9 %all_to_all.5.squares_ref = f32[16,1,128]{2,1,0:T(1,128)S(1)} all-to-all(f32[16,1,128]{2,1,0:T(1,128)S(1)} %get-tuple-element.40), channel_id=1, replica_groups=mesh['sp'=48,'tp'=16] {'tp'}, dimensions={0} | all-to-all | bytes 16384 | tf_op jit(solution)/shard_map/all_to_all | solution.py:349
  107.0 0.7 finish.1
  (5 shorter events, 0.0 us)
Async XLA Ops:
  19.8 9.1 %copy-start = (f32[2,2,15,31]{3,1,2,0:T(2,128)S(1)}, f32[2,2,15,31]{3,1,2,0:T(2,128)}, u32[]{:S(2)}) copy-start(f32[2,2,15,31]{3,1,2,0:T(2,128)} %param.15) | copy-start | bytes 22324
  21.4 9.5 %collective-permute-start = (bf16[144,256]{1,0:T(8,128)(2,1)S(1)}, bf16[144,256]{1,0:T(8,128)(2,1)S(1)}, u32[]{:S(2)}, u32[]{:S(2)}) collective-permute-start(bf16[144,256]{1,0:T(8,128)(2,1)S(1)} %get-tuple-element.27.own_ref), channel_id=1, source_target_pairs={{16,32},{32,16},{48,64},{64,48},{80,96},{96,80},{112,128},{128,112... | collective-permute-start | bytes 221192 | tf_op jit(solution)/shard_map/ppermute | solution.py:264
  27.0 5.1 %collective-permute-start.1 = (bf16[144,256]{1,0:T(8,128)(2,1)S(1)}, bf16[144,256]{1,0:T(8,128)(2,1)S(1)}, u32[]{:S(2)}, u32[]{:S(2)}) collective-permute-start(bf16[144,256]{1,0:T(8,128)(2,1)S(1)} %get-tuple-element.27.own_ref), channel_id=1, source_target_pairs={{0,16},{16,0},{32,48},{48,32},{64,80},{80,64},{96,112},{112,96},{1... | collective-permute-start | bytes 221192 | tf_op jit(solution)/shard_map/ppermute | solution.py:264
  68.3 8.7 %collective-permute-start.2 = (bf16[128,256]{1,0:T(8,128)(2,1)S(1)}, bf16[128,256]{1,0:T(8,128)(2,1)S(1)}, u32[]{:S(2)}, u32[]{:S(2)}) collective-permute-start(bf16[128,256]{1,0:T(8,128)(2,1)S(1)} %get-tuple-element.37.own_ref), channel_id=1, source_target_pairs={{16,32},{32,16},{48,64},{64,48},{80,96},{96,80},{112,128},{128,112... | collective-permute-start | bytes 196616 | tf_op jit(solution)/shard_map/ppermute | solution.py:264
  71.5 5.5 %collective-permute-start.3 = (bf16[128,256]{1,0:T(8,128)(2,1)S(1)}, bf16[128,256]{1,0:T(8,128)(2,1)S(1)}, u32[]{:S(2)}, u32[]{:S(2)}) collective-permute-start(bf16[128,256]{1,0:T(8,128)(2,1)S(1)} %get-tuple-element.37.own_ref), channel_id=1, source_target_pairs={{0,16},{16,0},{32,48},{48,32},{64,80},{80,64},{96,112},{112,96},{1... | collective-permute-start | bytes 196616 | tf_op jit(solution)/shard_map/ppermute | solution.py:264

commit v5 on v4

--- a/solution.py
+++ b/solution.py
@@ -221,11 +221,11 @@
     result = summed[:tokens]
     for h in range(1, heads):
         result = jnp.where(lane // HEAD_DIM == h, summed[lanes(h, tokens)], result)
-    out_ref[...] = result.astype(jnp.bfloat16)
+    out_ref[...] = jnp.broadcast_to(result.astype(jnp.bfloat16)[None], out_ref.shape)
 
 
 def projected(a_ref, w_ref):
-    joined = jnp.concatenate([a_ref[i] for i in range(a_ref.shape[0])], axis=1)
+    joined = jnp.concatenate([a_ref[place(i, a_ref.shape[0])] for i in range(a_ref.shape[0])], axis=1)
     return jnp.dot(joined, w_ref[...], preferred_element_type=jnp.float32)
 
 
@@ -266,6 +266,19 @@
 
 def gathered(block):
     return lax.all_gather(block, "tp", axis=0)
+
+
+def place(index, count):
+    return index % 2 * (count // 2) + index // 2
+
+
+def gathered_by_core(copies):
+    chips = copies.shape[0]
+    across = [[core + 2 * chip for chip in range(chips)] for core in range(2)]
+    pairs = [[2 * chip, 2 * chip + 1] for chip in range(chips)]
+    same = lax.all_to_all(copies, "tp", 0, 0, axis_index_groups=across, tiled=True)
+    both = lax.all_gather(same, "tp", axis=0, axis_index_groups=pairs)
+    return both.reshape(2 * chips, *copies.shape[1:])
 
 
 def shards(
@@ -316,11 +329,11 @@
     doc_rows = (cross[tokens:], kv[tokens:], within[tokens:])
 
     def attention(query, kv, cross, within, bias):
-        return call(attend, pltpu.VMEM((tokens, cols), bf16), [VMEM] * 8, "attend")(
+        return call(attend, pltpu.VMEM((members // 2, tokens, cols), bf16), [VMEM] * 8, "attend")(
             query, kv, cross, within, *doc_rows, bias
         )
 
-    attended = gathered(attention(query, kv, cross, within, bias))
+    attended = gathered_by_core(attention(query, kv, cross, within, bias))
     branch = call(first_out, pltpu.VMEM((tokens + PAD, feat), bf16), [VMEM] * 3, "first_out")(
         attended, out, post
     )
@@ -339,7 +352,7 @@
         "next_query",
         [weight, pltpu.SemaphoreType.DMA((2,))],
     )(scaled, scaler, flat, query_weight, out_weight)
-    attended = gathered(attention(query, kv, cross, within, bias))
+    attended = gathered_by_core(attention(query, kv, cross, within, bias))
     branch, squares = call(
         last_out,
         (pltpu.VMEM((tokens, feat), f32), pltpu.VMEM((members, 1, tokens), f32)),

time: 108 us -> 107 us (level)
  blocking collectives: 83.6 us -> 82.4 us
    all_gather x4 -> x2, blocking collectives: 71.8 us -> 36.3 us  [gathered(): return lax.all_gather(block, 'tp', axis=0)]
    all_to_all x0 -> x2, blocking collectives: none -> 26.3 us  [gathered_by_core(): lax.all_to_all(copies, 'tp', 0, 0, axis_index_groups=across, tiled=True)]
    all_gather x0 -> x2, blocking collectives: none -> 9.92 us  [gathered_by_core(): both = lax.all_gather(same, 'tp', axis=0, axis_index_groups=pairs)]
    all_to_all x1, blocking collectives: 11.9 us -> 9.85 us  [shards(): squares = lax.all_to_all(squares, 'tp', 0, 0, tiled=True)]
  transfers between devices with their start and end apart: 4 -> 4, of which waited for: 2 -> 3; matrix products, arithmetic and copies ran while one was open for 0% -> 0% of each run, Pallas kernels for 3% -> 3%
where the time goes in v5:
time: 107 us
  blocking collectives  82.4 us (77%)
  starting transfers between devices  13.2 us (12%)
  Pallas kernels  8.06 us (8%)
  waiting for transfers between devices  2.98 us (3%)
    all_gather x2, blocking collectives, gathered(): return lax.all_gather(block, 'tp', axis=0)  36.3 us
    all_to_all x2, blocking collectives, gathered_by_core(): lax.all_to_all(copies, 'tp', 0, 0, axis_index_groups=across, tiled=True)  26.3 us
    all_gather x2, blocking collectives, gathered_by_core(): both = lax.all_gather(same, 'tp', axis=0, axis_index_groups=pairs)  9.92 us
    all_to_all x1, blocking collectives, shards(): squares = lax.all_to_all(squares, 'tp', 0, 0, tiled=True)  9.85 us
    ppermute x2, starting transfers between devices, neighbours(): lax.ppermute(block, 'sp', crossing)  9.36 us
    pallas_call x9, Pallas kernels, run(): kernel(*(pltpu.with_memory_space_constraint(arg, spec.memory_space) for a...  8.06 us
    ppermute x2, starting transfers between devices, neighbours(): lax.ppermute(block, 'sp', within)  3.84 us
  transfers between devices with their start and end apart: 4, of which 3 were waited for; matrix products, arithmetic and copies ran while one was open for 0% of the time, Pallas kernels for 3%

profile of v5, /device:TPU:513, one launch (start us, length us, event | category | flops | bytes accessed | tf_op | source)
XLA Modules:
  0.0 106.9 jit_solution(2699783310682711601)
XLA Ops:
  0.0 19.8 %all-gather = bf16[2048,128]{1,0:T(8,128)(2,1)S(1)} all-gather(bf16[128,128]{1,0:T(8,128)(2,1)} %param.9), channel_id=2, replica_groups=mesh['sp'=48,'tp'=16] {'tp'}, dimensions={0}, use_global_device_ids=true | all-gather | bytes 557056 | tf_op jit(solution)/shard_map/all_gather | solution.py:268
  19.8 0.0 copy-start
  19.8 1.6 %first_heads.1 = (bf16[144,256]{1,0:T(8,128)(2,1)S(1)}, bf16[128,2048]{1,0:T(8,128)(2,1)S(1)}, f32[128,128]{1,0:T(8,128)S(1)}, f32[2,2048]{1,0:T(2,128)S(1)}) custom-call(bf16[16,128,128]{2,1,0:T(8,128)(2,1)S(1)} %bitcast.5, f32[2,2048]{1,0:T(2,128)} %gain_hbm.1, s32[1,128]{1,0:T(1,128)} %bitcast.8, bf16[2,2048,128]{2,1,0:T(8,128)(2,1)} %wk_hbm.3, ...), custom_call_target="tpu_custom_call" | custom-call | tf_op jit(solution)/shard_map/first_heads/pallas_call | solution.py:37
  21.4 5.6 %collective-permute-start = (bf16[144,256]{1,0:T(8,128)(2,1)S(1)}, bf16[144,256]{1,0:T(8,128)(2,1)S(1)}, u32[]{:S(2)}, u32[]{:S(2)}) collective-permute-start(bf16[144,256]{1,0:T(8,128)(2,1)S(1)} %get-tuple-element.27.own_ref), channel_id=1, source_target_pairs={{16,32},{32,16},{48,64},{64,48},{80,96},{96,80},{112,128},{128,112... | collective-permute-start | bytes 221192 | tf_op jit(solution)/shard_map/ppermute | solution.py:264
  27.0 1.9 %collective-permute-start.1 = (bf16[144,256]{1,0:T(8,128)(2,1)S(1)}, bf16[144,256]{1,0:T(8,128)(2,1)S(1)}, u32[]{:S(2)}, u32[]{:S(2)}) collective-permute-start(bf16[144,256]{1,0:T(8,128)(2,1)S(1)} %get-tuple-element.27.own_ref), channel_id=1, source_target_pairs={{0,16},{16,0},{32,48},{48,32},{64,80},{80,64},{96,112},{112,96},{1... | collective-permute-start | bytes 221192 | tf_op jit(solution)/shard_map/ppermute | solution.py:264
  28.9 0.0 copy-done
  28.9 0.1 reshape.13.flat_ref
  29.0 1.8 %first_query.1 = (bf16[128,128]{1,0:T(8,128)(2,1)S(1)}, f32[3,2,128,128]{3,2,1,0:T(8,128)S(1)}, bf16[2048,128]{1,0:T(8,128)(2,1)S(1)}, bf16[2048,128]{1,0:T(8,12...) custom-call(bf16[128,2048]{1,0:T(8,128)(2,1)S(1)} %get-tuple-element.24.scaled_ref, ...), custom_call_target="tpu_custom_call" | custom-call | tf_op jit(solution)/shard_map/first_query/pallas_call | solution.py:37
  30.8 0.0 collective-permute-done.cross_ref
  30.8 1.2 %collective-permute-done.1.within_ref = bf16[144,256]{1,0:T(8,128)(2,1)S(1)} collective-permute-done((bf16[144,256]{1,0:T(8,128)(2,1)S(1)}, bf16[144,256]{1,0:T(8,128)(2,1)S(1)}, u32[]{:S(2)}, u32[]{:S(2)}) %collective-permute-start.1) | collective-permute-done | bytes 73760 | tf_op jit(solution)/shard_map/ppermute | solution.py:264
  32.1 0.5 attend.2
  32.5 13.2 %all_to_all.15 = bf16[8,128,128]{2,1,0:T(8,128)(2,1)S(1)} all-to-all(bf16[8,128,128]{2,1,0:T(8,128)(2,1)S(1)} %attend.2), channel_id=1, replica_groups={{0,2,4,6,8,10,12,14},{1,3,5,7,9,11,13,15},{16,18,20,22,24,26,28,30},{17..., dimensions={0} | all-to-all | bytes 524288 | tf_op jit(solution)/shard_map/all_to_all | solution.py:279
  45.7 5.3 %all-gather.1.a_ref = bf16[16,128,128]{2,1,0:T(8,128)(2,1)S(1)} all-gather(bf16[8,128,128]{2,1,0:T(8,128)(2,1)S(1)} %all_to_all.15), channel_id=3, replica_groups={{0,1},{2,3},{4,5},{6,7},{8,9},{10,11},{12,13},{14,15},{16,17},{18,19},{..., dimensions={0}, use_global_device_ids=true | all-gather | bytes 786432 | tf_op jit(solution)/shard_map/all_gather | solution.py:280
  51.0 0.3 first_out.1
  51.3 16.5 %all-gather.2 = bf16[2304,128]{1,0:T(8,128)(2,1)S(1)} all-gather(bf16[144,128]{1,0:T(8,128)(2,1)S(1)} %first_out.1), channel_id=4, replica_groups=mesh['sp'=48,'tp'=16] {'tp'}, dimensions={0}, use_global_device_ids=true | all-gather | bytes 626688 | tf_op jit(solution)/shard_map/all_gather | solution.py:268
  67.8 0.8 next_heads.1
  68.5 3.8 %collective-permute-start.2 = (bf16[128,256]{1,0:T(8,128)(2,1)S(1)}, bf16[128,256]{1,0:T(8,128)(2,1)S(1)}, u32[]{:S(2)}, u32[]{:S(2)}) collective-permute-start(bf16[128,256]{1,0:T(8,128)(2,1)S(1)} %get-tuple-element.37.own_ref), channel_id=1, source_target_pairs={{16,32},{32,16},{48,64},{64,48},{80,96},{96,80},{112,128},{128,112... | collective-permute-start | bytes 196616 | tf_op jit(solution)/shard_map/ppermute | solution.py:264
  72.3 1.9 %collective-permute-start.3 = (bf16[128,256]{1,0:T(8,128)(2,1)S(1)}, bf16[128,256]{1,0:T(8,128)(2,1)S(1)}, u32[]{:S(2)}, u32[]{:S(2)}) collective-permute-start(bf16[128,256]{1,0:T(8,128)(2,1)S(1)} %get-tuple-element.37.own_ref), channel_id=1, source_target_pairs={{0,16},{16,0},{32,48},{48,32},{64,80},{80,64},{96,112},{112,96},{1... | collective-permute-start | bytes 196616 | tf_op jit(solution)/shard_map/ppermute | solution.py:264
  74.3 1.6 %next_query.1 = (bf16[128,128]{1,0:T(8,128)(2,1)S(1)}, f32[3,2,128,128]{3,2,1,0:T(8,128)S(1)}, bf16[2048,128]{1,0:T(8,128)(2,1)S(1)}) custom-call(bf16[128,2048]{1,0:T(8,128)(2,1)S(1)} %get-tuple-element.34.scaled_ref, f32[128,128]{1,0:T(8,128)S(1)} %get-tuple-element.35.scaler_ref, f32[2,2,512]{2,1,0:T(2,128)S(1)} %reshape.13.flat_ref, ...), custom_call_target="tpu_custom_call" | custom-call | tf_op jit(solution)/shard_map/next_query/pallas_call | solution.py:37
  75.9 1.4 %collective-permute-done.2.cross_ref = bf16[128,256]{1,0:T(8,128)(2,1)S(1)} collective-permute-done((bf16[128,256]{1,0:T(8,128)(2,1)S(1)}, bf16[128,256]{1,0:T(8,128)(2,1)S(1)}, u32[]{:S(2)}, u32[]{:S(2)}) %collective-permute-start.2) | collective-permute-done | bytes 65568 | tf_op jit(solution)/shard_map/ppermute | solution.py:264
  77.2 0.4 collective-permute-done.3.within_ref
  77.6 0.5 attend.3
  78.1 13.2 %all_to_all.16 = bf16[8,128,128]{2,1,0:T(8,128)(2,1)S(1)} all-to-all(bf16[8,128,128]{2,1,0:T(8,128)(2,1)S(1)} %attend.3), channel_id=1, replica_groups={{0,2,4,6,8,10,12,14},{1,3,5,7,9,11,13,15},{16,18,20,22,24,26,28,30},{17..., dimensions={0} | all-to-all | bytes 524288 | tf_op jit(solution)/shard_map/all_to_all | solution.py:279
  91.3 4.6 %all-gather.3.a_ref = bf16[16,128,128]{2,1,0:T(8,128)(2,1)S(1)} all-gather(bf16[8,128,128]{2,1,0:T(8,128)(2,1)S(1)} %all_to_all.16), channel_id=5, replica_groups={{0,1},{2,3},{4,5},{6,7},{8,9},{10,11},{12,13},{14,15},{16,17},{18,19},{..., dimensions={0}, use_global_device_ids=true | all-gather | bytes 786432 | tf_op jit(solution)/shard_map/all_gather | solution.py:280
  95.9 0.4 last_out.1
  96.3 9.8 %all_to_all.17.squares_ref = f32[16,1,128]{2,1,0:T(1,128)S(1)} all-to-all(f32[16,1,128]{2,1,0:T(1,128)S(1)} %get-tuple-element.40), channel_id=1, replica_groups=mesh['sp'=48,'tp'=16] {'tp'}, dimensions={0} | all-to-all | bytes 16384 | tf_op jit(solution)/shard_map/all_to_all | solution.py:362
  106.1 0.7 finish.1
  (5 shorter events, 0.0 us)
Async XLA Ops:
  19.8 9.1 %copy-start = (f32[2,2,15,31]{3,1,2,0:T(2,128)S(1)}, f32[2,2,15,31]{3,1,2,0:T(2,128)}, u32[]{:S(2)}) copy-start(f32[2,2,15,31]{3,1,2,0:T(2,128)} %param.15) | copy-start | bytes 22324
  21.4 9.5 %collective-permute-start = (bf16[144,256]{1,0:T(8,128)(2,1)S(1)}, bf16[144,256]{1,0:T(8,128)(2,1)S(1)}, u32[]{:S(2)}, u32[]{:S(2)}) collective-permute-start(bf16[144,256]{1,0:T(8,128)(2,1)S(1)} %get-tuple-element.27.own_ref), channel_id=1, source_target_pairs={{16,32},{32,16},{48,64},{64,48},{80,96},{96,80},{112,128},{128,112... | collective-permute-start | bytes 221192 | tf_op jit(solution)/shard_map/ppermute | solution.py:264
  27.0 5.1 %collective-permute-start.1 = (bf16[144,256]{1,0:T(8,128)(2,1)S(1)}, bf16[144,256]{1,0:T(8,128)(2,1)S(1)}, u32[]{:S(2)}, u32[]{:S(2)}) collective-permute-start(bf16[144,256]{1,0:T(8,128)(2,1)S(1)} %get-tuple-element.27.own_ref), channel_id=1, source_target_pairs={{0,16},{16,0},{32,48},{48,32},{64,80},{80,64},{96,112},{112,96},{1... | collective-permute-start | bytes 221192 | tf_op jit(solution)/shard_map/ppermute | solution.py:264
  68.5 8.7 %collective-permute-start.2 = (bf16[128,256]{1,0:T(8,128)(2,1)S(1)}, bf16[128,256]{1,0:T(8,128)(2,1)S(1)}, u32[]{:S(2)}, u32[]{:S(2)}) collective-permute-start(bf16[128,256]{1,0:T(8,128)(2,1)S(1)} %get-tuple-element.37.own_ref), channel_id=1, source_target_pairs={{16,32},{32,16},{48,64},{64,48},{80,96},{96,80},{112,128},{128,112... | collective-permute-start | bytes 196616 | tf_op jit(solution)/shard_map/ppermute | solution.py:264
  72.3 5.3 %collective-permute-start.3 = (bf16[128,256]{1,0:T(8,128)(2,1)S(1)}, bf16[128,256]{1,0:T(8,128)(2,1)S(1)}, u32[]{:S(2)}, u32[]{:S(2)}) collective-permute-start(bf16[128,256]{1,0:T(8,128)(2,1)S(1)} %get-tuple-element.37.own_ref), channel_id=1, source_target_pairs={{0,16},{16,0},{32,48},{48,32},{64,80},{80,64},{96,112},{112,96},{1... | collective-permute-start | bytes 196616 | tf_op jit(solution)/shard_map/ppermute | solution.py:264

commit v6 on v5

--- a/solution.py
+++ b/solution.py
@@ -17,6 +17,7 @@
 BIAS_ROWS = 2 * WIN_ROWS
 LOWEST = -1e30
 PAD = 16
+CHUNKS = 2
 
 VMEM = pl.BlockSpec(memory_space=pltpu.VMEM)
 HBM = pl.BlockSpec(memory_space=pltpu.HBM)
@@ -75,31 +76,44 @@
     x_ref, gain_hbm, docs_hbm, wk_hbm, wv_hbm,
     kv_ref, scaled_ref, scaler_ref, gain_ref, docs_ref, wk_ref, wv_ref, sems,
 ):
-    copies = copying(
+    count, tokens, feat = x_ref.shape
+    cols = wk_ref.shape[1]
+    step = count * feat // CHUNKS
+    pieces = [slice(i * step, (i + 1) * step) for i in range(CHUNKS)]
+    gain_copy, *copies, docs_copy = copying(
         (
             (gain_hbm, gain_ref),
+            *(
+                (hbm.at[0, piece], ref.at[piece])
+                for piece in pieces
+                for hbm, ref in ((wk_hbm, wk_ref), (wv_hbm, wv_ref))
+            ),
             (docs_hbm, docs_ref),
-            (wk_hbm.at[0], wk_ref),
-            (wv_hbm.at[0], wv_ref),
         ),
         sems,
     )
-    count, tokens, feat = x_ref.shape
     squares = jnp.zeros((tokens, feat), jnp.float32)
-    copies[0].wait()
     for i in range(count):
         wide = x_ref[i].astype(jnp.float32)
         squares += wide * wide
-        scaled_ref[:, lanes(i, feat)] = (wide * gain_ref[0:1, lanes(i, feat)]).astype(jnp.bfloat16)
     scaler = scaler_of(squares, count * feat)
     scaler_ref[...] = scaler
-    copies[1].wait()
+    gain_copy.wait()
+    for i in range(count):
+        wide = x_ref[i].astype(jnp.float32)
+        scaled_ref[:, lanes(i, feat)] = (wide * gain_ref[0:1, lanes(i, feat)]).astype(jnp.bfloat16)
+    both = jnp.zeros((tokens, 2 * cols), jnp.float32)
+    for i, piece in enumerate(pieces):
+        copies[2 * i].wait()
+        copies[2 * i + 1].wait()
+        weights = jnp.concatenate([wk_ref[piece], wv_ref[piece]], axis=1)
+        both += jnp.dot(scaled_ref[:, piece], weights, preferred_element_type=jnp.float32)
+    scaler = jnp.concatenate([scaler] * (2 * cols // feat), axis=1)
+    kv_ref[:tokens] = (both * scaler).astype(jnp.bfloat16)
+    docs_copy.wait()
     row = docs_ref[...].astype(jnp.float32)
     row = jnp.concatenate([row] * (kv_ref.shape[1] // tokens), axis=1)
     kv_ref[tokens:] = jnp.broadcast_to(row, (kv_ref.shape[0] - tokens, kv_ref.shape[1])).astype(jnp.bfloat16)
-    copies[2].wait()
-    copies[3].wait()
-    key_value(scaled_ref[...], scaler, wk_ref[...], wv_ref[...], kv_ref)
 
 
 def query_from(scaled_ref, scaler_ref, wq):
@@ -310,7 +324,7 @@
         (pltpu.VMEM((tokens + PAD, 2 * cols), bf16), *shared, pltpu.VMEM(pre_gain.shape, f32)),
         [VMEM] + [HBM] * 4,
         "first_heads",
-        [pltpu.VMEM((1, tokens), jnp.int32), weight, weight, pltpu.SemaphoreType.DMA((4,))],
+        [pltpu.VMEM((1, tokens), jnp.int32), weight, weight, pltpu.SemaphoreType.DMA((2 + 2 * CHUNKS,))],
     )(stream, pre_gain, documents.reshape(1, tokens), key_weight, value_weight)
     cross, within = neighbours(kv)
     bias_of = pltpu.VMEM((3, heads, tokens, tokens), f32)

time: 107 us -> 107 us (level)
  no operation moved by 1% of the time
where the time goes in v6:
time: 107 us
  blocking collectives  82.4 us (77%)
  starting transfers between devices  13.2 us (12%)
  Pallas kernels  8.04 us (8%)
  waiting for transfers between devices  2.98 us (3%)
    all_gather x2, blocking collectives, gathered(): return lax.all_gather(block, 'tp', axis=0)  36.3 us
    all_to_all x2, blocking collectives, gathered_by_core(): lax.all_to_all(copies, 'tp', 0, 0, axis_index_groups=across, tiled=True)  26.3 us
    all_gather x2, blocking collectives, gathered_by_core(): both = lax.all_gather(same, 'tp', axis=0, axis_index_groups=pairs)  9.95 us
    all_to_all x1, blocking collectives, shards(): squares = lax.all_to_all(squares, 'tp', 0, 0, tiled=True)  9.85 us
    ppermute x2, starting transfers between devices, neighbours(): lax.ppermute(block, 'sp', crossing)  9.36 us
    pallas_call x9, Pallas kernels, run(): kernel(*(pltpu.with_memory_space_constraint(arg, spec.memory_space) for a...  8.04 us
    ppermute x2, starting transfers between devices, neighbours(): lax.ppermute(block, 'sp', within)  3.84 us
  transfers between devices with their start and end apart: 4, of which 3 were waited for; matrix products, arithmetic and copies ran while one was open for 0% of the time, Pallas kernels for 3%

profile of v6, /device:TPU:513, one launch (start us, length us, event | category | flops | bytes accessed | tf_op | source)
XLA Modules:
  0.0 106.8 jit_solution(13976357640488237295)
XLA Ops:
  0.0 19.8 %all-gather = bf16[2048,128]{1,0:T(8,128)(2,1)S(1)} all-gather(bf16[128,128]{1,0:T(8,128)(2,1)} %param.9), channel_id=2, replica_groups=mesh['sp'=48,'tp'=16] {'tp'}, dimensions={0}, use_global_device_ids=true | all-gather | bytes 557056 | tf_op jit(solution)/shard_map/all_gather | solution.py:282
  19.8 0.0 copy-start
  19.8 1.6 %first_heads.1 = (bf16[144,256]{1,0:T(8,128)(2,1)S(1)}, bf16[128,2048]{1,0:T(8,128)(2,1)S(1)}, f32[128,128]{1,0:T(8,128)S(1)}, f32[2,2048]{1,0:T(2,128)S(1)}) custom-call(bf16[16,128,128]{2,1,0:T(8,128)(2,1)S(1)} %bitcast.5, f32[2,2048]{1,0:T(2,128)} %gain_hbm.1, s32[1,128]{1,0:T(1,128)} %bitcast.8, bf16[2,2048,128]{2,1,0:T(8,128)(2,1)} %wk_hbm.3, ...), custom_call_target="tpu_custom_call" | custom-call | tf_op jit(solution)/shard_map/first_heads/pallas_call | solution.py:38
  21.4 5.6 %collective-permute-start = (bf16[144,256]{1,0:T(8,128)(2,1)S(1)}, bf16[144,256]{1,0:T(8,128)(2,1)S(1)}, u32[]{:S(2)}, u32[]{:S(2)}) collective-permute-start(bf16[144,256]{1,0:T(8,128)(2,1)S(1)} %get-tuple-element.27.own_ref), channel_id=1, source_target_pairs={{16,32},{32,16},{48,64},{64,48},{80,96},{96,80},{112,128},{128,112... | collective-permute-start | bytes 221192 | tf_op jit(solution)/shard_map/ppermute | solution.py:278
  26.9 1.9 %collective-permute-start.1 = (bf16[144,256]{1,0:T(8,128)(2,1)S(1)}, bf16[144,256]{1,0:T(8,128)(2,1)S(1)}, u32[]{:S(2)}, u32[]{:S(2)}) collective-permute-start(bf16[144,256]{1,0:T(8,128)(2,1)S(1)} %get-tuple-element.27.own_ref), channel_id=1, source_target_pairs={{0,16},{16,0},{32,48},{48,32},{64,80},{80,64},{96,112},{112,96},{1... | collective-permute-start | bytes 221192 | tf_op jit(solution)/shard_map/ppermute | solution.py:278
  28.9 0.0 copy-done
  28.9 0.1 reshape.13.flat_ref
  29.0 1.8 %first_query.1 = (bf16[128,128]{1,0:T(8,128)(2,1)S(1)}, f32[3,2,128,128]{3,2,1,0:T(8,128)S(1)}, bf16[2048,128]{1,0:T(8,128)(2,1)S(1)}, bf16[2048,128]{1,0:T(8,12...) custom-call(bf16[128,2048]{1,0:T(8,128)(2,1)S(1)} %get-tuple-element.24.scaled_ref, ...), custom_call_target="tpu_custom_call" | custom-call | tf_op jit(solution)/shard_map/first_query/pallas_call | solution.py:38
  30.8 0.0 collective-permute-done.cross_ref
  30.8 1.2 %collective-permute-done.1.within_ref = bf16[144,256]{1,0:T(8,128)(2,1)S(1)} collective-permute-done((bf16[144,256]{1,0:T(8,128)(2,1)S(1)}, bf16[144,256]{1,0:T(8,128)(2,1)S(1)}, u32[]{:S(2)}, u32[]{:S(2)}) %collective-permute-start.1) | collective-permute-done | bytes 73760 | tf_op jit(solution)/shard_map/ppermute | solution.py:278
  32.0 0.5 attend.2
  32.5 13.1 %all_to_all.15 = bf16[8,128,128]{2,1,0:T(8,128)(2,1)S(1)} all-to-all(bf16[8,128,128]{2,1,0:T(8,128)(2,1)S(1)} %attend.2), channel_id=1, replica_groups={{0,2,4,6,8,10,12,14},{1,3,5,7,9,11,13,15},{16,18,20,22,24,26,28,30},{17..., dimensions={0} | all-to-all | bytes 524288 | tf_op jit(solution)/shard_map/all_to_all | solution.py:293
  45.6 5.3 %all-gather.1.a_ref = bf16[16,128,128]{2,1,0:T(8,128)(2,1)S(1)} all-gather(bf16[8,128,128]{2,1,0:T(8,128)(2,1)S(1)} %all_to_all.15), channel_id=3, replica_groups={{0,1},{2,3},{4,5},{6,7},{8,9},{10,11},{12,13},{14,15},{16,17},{18,19},{..., dimensions={0}, use_global_device_ids=true | all-gather | bytes 786432 | tf_op jit(solution)/shard_map/all_gather | solution.py:294
  51.0 0.3 first_out.1
  51.3 16.5 %all-gather.2 = bf16[2304,128]{1,0:T(8,128)(2,1)S(1)} all-gather(bf16[144,128]{1,0:T(8,128)(2,1)S(1)} %first_out.1), channel_id=4, replica_groups=mesh['sp'=48,'tp'=16] {'tp'}, dimensions={0}, use_global_device_ids=true | all-gather | bytes 626688 | tf_op jit(solution)/shard_map/all_gather | solution.py:282
  67.8 0.7 next_heads.1
  68.5 3.8 %collective-permute-start.2 = (bf16[128,256]{1,0:T(8,128)(2,1)S(1)}, bf16[128,256]{1,0:T(8,128)(2,1)S(1)}, u32[]{:S(2)}, u32[]{:S(2)}) collective-permute-start(bf16[128,256]{1,0:T(8,128)(2,1)S(1)} %get-tuple-element.37.own_ref), channel_id=1, source_target_pairs={{16,32},{32,16},{48,64},{64,48},{80,96},{96,80},{112,128},{128,112... | collective-permute-start | bytes 196616 | tf_op jit(solution)/shard_map/ppermute | solution.py:278
  72.3 1.9 %collective-permute-start.3 = (bf16[128,256]{1,0:T(8,128)(2,1)S(1)}, bf16[128,256]{1,0:T(8,128)(2,1)S(1)}, u32[]{:S(2)}, u32[]{:S(2)}) collective-permute-start(bf16[128,256]{1,0:T(8,128)(2,1)S(1)} %get-tuple-element.37.own_ref), channel_id=1, source_target_pairs={{0,16},{16,0},{32,48},{48,32},{64,80},{80,64},{96,112},{112,96},{1... | collective-permute-start | bytes 196616 | tf_op jit(solution)/shard_map/ppermute | solution.py:278
  74.2 1.6 %next_query.1 = (bf16[128,128]{1,0:T(8,128)(2,1)S(1)}, f32[3,2,128,128]{3,2,1,0:T(8,128)S(1)}, bf16[2048,128]{1,0:T(8,128)(2,1)S(1)}) custom-call(bf16[128,2048]{1,0:T(8,128)(2,1)S(1)} %get-tuple-element.34.scaled_ref, f32[128,128]{1,0:T(8,128)S(1)} %get-tuple-element.35.scaler_ref, f32[2,2,512]{2,1,0:T(2,128)S(1)} %reshape.13.flat_ref, ...), custom_call_target="tpu_custom_call" | custom-call | tf_op jit(solution)/shard_map/next_query/pallas_call | solution.py:38
  75.8 1.4 %collective-permute-done.2.cross_ref = bf16[128,256]{1,0:T(8,128)(2,1)S(1)} collective-permute-done((bf16[128,256]{1,0:T(8,128)(2,1)S(1)}, bf16[128,256]{1,0:T(8,128)(2,1)S(1)}, u32[]{:S(2)}, u32[]{:S(2)}) %collective-permute-start.2) | collective-permute-done | bytes 65568 | tf_op jit(solution)/shard_map/ppermute | solution.py:278
  77.2 0.4 collective-permute-done.3.within_ref
  77.6 0.5 attend.3
  78.1 13.2 %all_to_all.16 = bf16[8,128,128]{2,1,0:T(8,128)(2,1)S(1)} all-to-all(bf16[8,128,128]{2,1,0:T(8,128)(2,1)S(1)} %attend.3), channel_id=1, replica_groups={{0,2,4,6,8,10,12,14},{1,3,5,7,9,11,13,15},{16,18,20,22,24,26,28,30},{17..., dimensions={0} | all-to-all | bytes 524288 | tf_op jit(solution)/shard_map/all_to_all | solution.py:293
  91.2 4.6 %all-gather.3.a_ref = bf16[16,128,128]{2,1,0:T(8,128)(2,1)S(1)} all-gather(bf16[8,128,128]{2,1,0:T(8,128)(2,1)S(1)} %all_to_all.16), channel_id=5, replica_groups={{0,1},{2,3},{4,5},{6,7},{8,9},{10,11},{12,13},{14,15},{16,17},{18,19},{..., dimensions={0}, use_global_device_ids=true | all-gather | bytes 786432 | tf_op jit(solution)/shard_map/all_gather | solution.py:294
  95.9 0.4 last_out.1
  96.2 9.8 %all_to_all.17.squares_ref = f32[16,1,128]{2,1,0:T(1,128)S(1)} all-to-all(f32[16,1,128]{2,1,0:T(1,128)S(1)} %get-tuple-element.40), channel_id=1, replica_groups=mesh['sp'=48,'tp'=16] {'tp'}, dimensions={0} | all-to-all | bytes 16384 | tf_op jit(solution)/shard_map/all_to_all | solution.py:376
  106.1 0.7 finish.1
  (5 shorter events, 0.0 us)
Async XLA Ops:
  19.8 9.1 %copy-start = (f32[2,2,15,31]{3,1,2,0:T(2,128)S(1)}, f32[2,2,15,31]{3,1,2,0:T(2,128)}, u32[]{:S(2)}) copy-start(f32[2,2,15,31]{3,1,2,0:T(2,128)} %param.15) | copy-start | bytes 22324
  21.4 9.5 %collective-permute-start = (bf16[144,256]{1,0:T(8,128)(2,1)S(1)}, bf16[144,256]{1,0:T(8,128)(2,1)S(1)}, u32[]{:S(2)}, u32[]{:S(2)}) collective-permute-start(bf16[144,256]{1,0:T(8,128)(2,1)S(1)} %get-tuple-element.27.own_ref), channel_id=1, source_target_pairs={{16,32},{32,16},{48,64},{64,48},{80,96},{96,80},{112,128},{128,112... | collective-permute-start | bytes 221192 | tf_op jit(solution)/shard_map/ppermute | solution.py:278
  26.9 5.1 %collective-permute-start.1 = (bf16[144,256]{1,0:T(8,128)(2,1)S(1)}, bf16[144,256]{1,0:T(8,128)(2,1)S(1)}, u32[]{:S(2)}, u32[]{:S(2)}) collective-permute-start(bf16[144,256]{1,0:T(8,128)(2,1)S(1)} %get-tuple-element.27.own_ref), channel_id=1, source_target_pairs={{0,16},{16,0},{32,48},{48,32},{64,80},{80,64},{96,112},{112,96},{1... | collective-permute-start | bytes 221192 | tf_op jit(solution)/shard_map/ppermute | solution.py:278
  68.5 8.7 %collective-permute-start.2 = (bf16[128,256]{1,0:T(8,128)(2,1)S(1)}, bf16[128,256]{1,0:T(8,128)(2,1)S(1)}, u32[]{:S(2)}, u32[]{:S(2)}) collective-permute-start(bf16[128,256]{1,0:T(8,128)(2,1)S(1)} %get-tuple-element.37.own_ref), channel_id=1, source_target_pairs={{16,32},{32,16},{48,64},{64,48},{80,96},{96,80},{112,128},{128,112... | collective-permute-start | bytes 196616 | tf_op jit(solution)/shard_map/ppermute | solution.py:278
  72.3 5.3 %collective-permute-start.3 = (bf16[128,256]{1,0:T(8,128)(2,1)S(1)}, bf16[128,256]{1,0:T(8,128)(2,1)S(1)}, u32[]{:S(2)}, u32[]{:S(2)}) collective-permute-start(bf16[128,256]{1,0:T(8,128)(2,1)S(1)} %get-tuple-element.37.own_ref), channel_id=1, source_target_pairs={{0,16},{16,0},{32,48},{48,32},{64,80},{80,64},{96,112},{112,96},{1... | collective-permute-start | bytes 196616 | tf_op jit(solution)/shard_map/ppermute | solution.py:278
